TPU v7x, 128 devices: a whole 4x4x4 slice. The times are simulated.
128 devices in a mesh: dp: 4 (over x), kv: 16 (over z, y), tp: 2 (over core).
Axes of the slice: x: 4, y: 4, z: 4, core: 2. Of those that a mesh axis runs over, the one named last changes fastest.
Arguments:
- tokens: bfloat16 [8192, 2048], P('dp', 'kv'), may hold values from -70 to 70
- pre_gain: float32 [2048], replicated, may hold values from 0.1 to 1.9
- query_weight: bfloat16 [2048, 1024], P(None, 'tp'), may hold values from -0.125 to 0.125
- key_weight: bfloat16 [2048, 1024], P(None, 'tp'), may hold values from -0.125 to 0.125
- value_weight: bfloat16 [2048, 1024], P(None, 'tp'), may hold values from -0.125 to 0.125
- gate_weight: bfloat16 [2048, 1024], P(None, 'tp'), may hold values from -0.125 to 0.125
- beta_weight: bfloat16 [2048, 8], replicated, may hold values from -0.125 to 0.125
- decay_weight: bfloat16 [2048, 8], replicated, may hold values from -0.125 to 0.125
- decay_log: float32 [8], P('tp'), may hold values from -3 to 0.5
- head_gain: float32 [128], replicated, may hold values from 0.1 to 1.9
- out_weight: bfloat16 [1024, 2048], P('tp', 'kv'), may hold values from -1 to 1
- post_gain: float32 [2048], P(('kv', 'tp')), may hold values from 0.1 to 1.9
- saved_state: float32 [2048, 8, 128, 128], P(('dp', 'kv'), 'tp'), may hold values from -4 to 4
- earlier_keys: bfloat16 [2048, 4, 8, 128], P(('dp', 'kv'), None, 'tp'), may hold values from -6 to 6
- earlier_values: bfloat16 [2048, 4, 8, 128], P(('dp', 'kv'), None, 'tp'), may hold values from -6 to 6
- earlier_rates: float32 [2048, 4, 8], P(('dp', 'kv'), None, 'tp'), may hold values from 0.05 to 0.95
- earlier_decays: float32 [2048, 4, 8], P(('dp', 'kv'), None, 'tp'), may hold values from -1.5 to -0.02
- accepted: int32 [2048], P(('dp', 'kv')), may hold values from 0 to 4
Outputs:
- mixed: bfloat16 [8192, 2048], P('dp', ('kv', 'tp'))
- committed: float32 [2048, 8, 128, 128], P(('dp', 'kv'), 'tp')
All inputs are finite; a program needn't handle non-finite values.
Results may differ from a plain program's by a relative error of at most 0.011.
Values may be sent and summed in bfloat16 or wider, within the bound.
A program may use at most 128 MiB of HBM per device.

v0:
```python
import jax
import jax.numpy as jnp
from jax import lax
from jax.sharding import PartitionSpec as P


def in_order(tiles, dim):
    dims = list(tiles.shape[1:])
    dims[dim] *= tiles.shape[0]
    return jnp.moveaxis(tiles, 0, dim).reshape(dims)


def from_everyone(shard, axis):
    count = lax.axis_size(axis)
    return lax.all_to_all(
        jnp.broadcast_to(shard[None], (count, *shard.shape)), axis, 0, 0, tiled=True
    )


def collect(shard, axis, dim):
    return in_order(from_everyone(shard, axis), dim)


def cut_along(shard, dim, count):
    before, after = (shard.shape[:dim], shard.shape[dim + 1 :])
    return jnp.moveaxis(shard.reshape(*before, count, -1, *after), dim, 0)


def summed_on_arrival(shard, axis, dim):
    count = lax.axis_size(axis)
    tiles = lax.all_to_all(cut_along(shard, dim, count), axis, 0, 0, tiled=True)
    return jnp.sum(tiles.astype(jnp.float32), axis=0)


def taken_together(shard, axis):
    everything = from_everyone(shard, axis)
    return jnp.sum(everything, axis=0)


def unit_norm(values):
    return values * lax.rsqrt(jnp.sum(values * values, axis=-1, keepdims=True) + 1e-06)


def advance(current, key_row, value_row, rate_now, log_decay):
    recalled = jnp.sum(key_row[..., :, None] * current, axis=-2)
    rate_cube = rate_now[..., None, None]
    current = current - rate_cube * key_row[..., :, None] * recalled[..., None, :]
    return (
        jnp.exp(log_decay)[..., None, None] * current
        + rate_cube * key_row[..., :, None] * value_row[..., None, :]
    )


def run_heads(
    saved_state,
    earlier_keys,
    earlier_values,
    earlier_rates,
    earlier_decays,
    accepted,
    queries,
    keys_unit,
    values_act,
    rates,
    decays,
):
    current = saved_state
    proposals = earlier_keys.shape[1]
    for position in range(proposals):
        live = (position < accepted).astype(jnp.float32)
        live = live.reshape(live.shape + (1,) * (earlier_rates.ndim - 2))
        current = advance(
            current,
            earlier_keys[:, position],
            earlier_values[:, position],
            earlier_rates[:, position] * live,
            earlier_decays[:, position] * live,
        )
    committed = current
    outputs = []
    for position in range(proposals):
        current = advance(
            current,
            keys_unit[:, position],
            values_act[:, position],
            rates[:, position],
            decays[:, position],
        )
        outputs.append(jnp.sum(queries[:, position][..., :, None] * current, axis=-2))
    return (committed, jnp.stack(outputs, axis=1))


def local(
    tokens,
    pre_gain,
    query_weight,
    key_weight,
    value_weight,
    gate_weight,
    beta_weight,
    decay_weight,
    decay_log,
    head_gain,
    out_weight,
    post_gain,
    saved_state,
    earlier_keys,
    earlier_values,
    earlier_rates,
    earlier_decays,
    accepted,
):
    seq_local = saved_state.shape[0]
    heads_local = saved_state.shape[1]
    head_size = saved_state.shape[2]
    proposals = earlier_keys.shape[1]
    rows_local = seq_local * proposals
    width_local = heads_local * head_size
    model_width = pre_gain.shape[0]
    head_start = lax.axis_index("tp") * heads_local
    beta_cols = lax.dynamic_slice_in_dim(beta_weight, head_start, heads_local, 1)
    decay_cols = lax.dynamic_slice_in_dim(decay_weight, head_start, heads_local, 1)
    own_rows = lax.all_to_all(tokens, "kv", split_axis=0, concat_axis=1, tiled=True)
    widened = own_rows.astype(jnp.float32)
    inverse = lax.rsqrt(jnp.mean(widened * widened, axis=1) + 1e-06)
    scaled = (widened * pre_gain).astype(jnp.bfloat16)
    stacked = jnp.stack(
        [
            jnp.dot(scaled, weight, preferred_element_type=jnp.float32)
            for weight in (query_weight, key_weight, value_weight, gate_weight)
        ],
        axis=1,
    )
    scalars = jnp.stack(
        [
            jnp.dot(scaled, cols, preferred_element_type=jnp.float32)
            for cols in (beta_cols, decay_cols)
        ],
        axis=1,
    )
    stacked = stacked * inverse[:, None, None]
    scalars = scalars * inverse[:, None, None]

    def heads_of(values):
        return values.reshape(seq_local, proposals, heads_local, head_size)

    queries = unit_norm(jax.nn.silu(heads_of(stacked[:, 0]))) * head_size ** (-0.5)
    keys_unit = unit_norm(jax.nn.silu(heads_of(stacked[:, 1])))
    values_act = jax.nn.silu(heads_of(stacked[:, 2]))
    gates_raw = heads_of(stacked[:, 3])
    rates = jax.nn.sigmoid(scalars[:, 0]).reshape(seq_local, proposals, heads_local)
    decays = -jnp.exp(decay_log) * jax.nn.softplus(scalars[:, 1]).reshape(
        seq_local, proposals, heads_local
    )
    committed, reads = run_heads(
        saved_state,
        unit_norm(earlier_keys.astype(jnp.float32)),
        earlier_values.astype(jnp.float32),
        earlier_rates,
        earlier_decays,
        accepted,
        queries,
        keys_unit,
        values_act,
        rates,
        decays,
    )
    normed = reads * lax.rsqrt(jnp.mean(reads * reads, axis=-1, keepdims=True) + 1e-06) * head_gain
    attended = (
        (normed * jax.nn.silu(gates_raw)).reshape(rows_local, width_local).astype(jnp.bfloat16)
    )
    partial_value = jnp.dot(
        collect(attended, "kv", 0), out_weight, preferred_element_type=jnp.float32
    )
    column_part = summed_on_arrival(partial_value.astype(jnp.bfloat16), "tp", 1)
    totals = taken_together(jnp.sum(column_part * column_part, axis=1), ("kv", "tp"))
    factor = lax.rsqrt(totals / model_width + 1e-06)
    mixed = (column_part * factor[:, None] * post_gain).astype(jnp.bfloat16)
    return (mixed, committed)


def solution(mesh):
    placed = (
        P("dp", "kv"),
        P(),
        P(None, "tp"),
        P(None, "tp"),
        P(None, "tp"),
        P(None, "tp"),
        P(),
        P(),
        P("tp"),
        P(),
        P("tp", "kv"),
        P(("kv", "tp")),
        P(("dp", "kv"), "tp", None, None),
        P(("dp", "kv"), None, "tp", None),
        P(("dp", "kv"), None, "tp", None),
        P(("dp", "kv"), None, "tp"),
        P(("dp", "kv"), None, "tp"),
        P(("dp", "kv")),
    )
    return jax.shard_map(
        local,
        mesh=mesh,
        in_specs=placed,
        out_specs=(P("dp", ("kv", "tp")), P(("dp", "kv"), "tp", None, None)),
        check_vma=False,
    )
```

profile of v0, /device:TPU:1, one launch (start us, length us, event | category | flops | bytes accessed | tf_op | source)
XLA Modules:
  0.0 188.4 jit_solution(10314389959742774240)
XLA Ops:
  0.6 8.7 %all-to-all-start = ((bf16[16,128,128]{2,1,0:T(8,128)(2,1)}), bf16[16,128,128]{2,1,0:T(8,128)(2,1)S(1)}, u32[]{:S(2)}, u32[]{:S(2)}) async-start(bf16[16,128,128]{2,1,0:T(8,128)(2,1)} %bitcast.154), calls=%async_computation | async-start | bytes 1048576 | tf_op jit(solution)/shard_map/all_to_all | solution.py:123
  9.4 0.7 exponential_negate_fusion
  10.1 1.2 broadcast_bitcast_fusion
  11.3 0.7 compare_convert_fusion.3
  12.0 0.8 bitcast_multiply_fusion.2
  13.5 1.1 fusion.40
  14.6 1.1 convert_multiply_fusion.1
  15.7 0.9 convert_element_type.60
  17.0 9.6 %multiply_add_fusion.6 = f32[32,4,128,128]{3,2,1,0:T(8,128)S(1)} fusion(f32[32,4,128,128]{3,2,1,0:T(8,128)} %param.30, f32[32,4,128]{2,1,0:T(4,128)S(1)} %get-tuple-element.34, f32[32,4,128]{2,1,0:T(4,128)S(1)} %get-tuple-element.30, f32[32,4]{1,0:T(8,128)S(1)} %copy.100, f32[32,4,128]{2,1,0:T(4,128)S(1)} %get-tuple-element.65), kind=kOutput, calls=%fused_computation.32 | output fusion | flops 12599423 | bytes 16974336 | tf_op jit(solution)/shard_map/mul | solution.py:47
  26.6 15.4 %multiply_add_fusion.5 = f32[32,4,128,128]{3,2,1,0:T(8,128)S(1)} fusion(f32[32,4,128,128]{3,2,1,0:T(8,128)S(1)} %multiply_add_fusion.6, f32[32,4,128]{2,1,0:T(4,128)S(1)} %get-tuple-element.33, f32[32,4,128]{2,1,0:T(4,128)S(1)} %get-tuple-element.29, f32[32,4]{1,0:T(8,128)S(1)} %copy.99, f32[32,4,128]{2,1,0:T(4,128)S(1)} %get-tuple-element.66), kind=kOutput, calls=%fused_computation.29 | output fusion | flops 12599423 | bytes 16974336 | tf_op jit(solution)/shard_map/mul | solution.py:47
  42.0 15.4 %multiply_add_fusion.4 = f32[32,4,128,128]{3,2,1,0:T(8,128)S(1)} fusion(f32[32,4,128,128]{3,2,1,0:T(8,128)S(1)} %multiply_add_fusion.5, f32[32,4,128]{2,1,0:T(4,128)S(1)} %get-tuple-element.32, f32[32,4,128]{2,1,0:T(4,128)S(1)} %get-tuple-element.28, f32[32,4]{1,0:T(8,128)S(1)} %copy.98, f32[32,4,128]{2,1,0:T(4,128)S(1)} %get-tuple-element.67), kind=kOutput, calls=%fused_computation.26 | output fusion | flops 12599423 | bytes 16974336 | tf_op jit(solution)/shard_map/mul | solution.py:47
  57.5 7.1 %multiply_add_fusion.3 = f32[32,4,128,128]{3,2,1,0:T(8,128)} fusion(f32[32,4,128,128]{3,2,1,0:T(8,128)S(1)} %multiply_add_fusion.4, f32[32,4,128]{2,1,0:T(4,128)S(1)} %get-tuple-element.31, f32[32,4,128]{2,1,0:T(4,128)S(1)} %get-tuple-element.27, f32[32,4]{1,0:T(8,128)S(1)} %copy.97, f32[32,4,128]{2,1,0:T(4,128)S(1)} %get-tuple-element.68), kind=kOutput, calls=%fused_computation.23 | output fusion | flops 12599423 | bytes 16974336 | tf_op jit(solution)/shard_map/mul | solution.py:47
  64.8 1.1 convert_bitcast_fusion
  65.9 2.6 %copy.95 = f32[128,16,128]{0,2,1:T(8,128)} copy(f32[128,16,128]{2,0,1:T(8,128)} %convert_bitcast_fusion) | data formatting | bytes 2097152 | tf_op jit(solution)/shard_map/convert_element_type | solution.py:124
  68.5 1.6 fusion.39
  72.6 0.9 copy.117
  73.4 0.9 copy.115
  74.3 0.9 copy.113
  75.2 0.5 convolution_bitcast_fusion
  75.7 2.2 %convolution_bitcast_fusion.1 = f32[128,1,512]{2,0,1:T(8,128)S(1)} fusion(bf16[128,2048]{0,1:T(8,128)(2,1)S(1)} %fusion.39, bf16[2048,512]{1,0:T(8,128)(2,1)} %param.22), kind=kOutput, calls=%fused_computation.47 | convolution fusion | flops 268435456 | bytes 2883584 | tf_op jit(solution)/shard_map/dot_general | solution.py:129
  77.9 2.1 %convolution_bitcast_fusion.2 = f32[128,1,512]{2,0,1:T(8,128)S(1)} fusion(bf16[128,2048]{0,1:T(8,128)(2,1)S(1)} %fusion.39, bf16[2048,512]{1,0:T(8,128)(2,1)} %param.21), kind=kOutput, calls=%fused_computation.48 | convolution fusion | flops 268435456 | bytes 2883584 | tf_op jit(solution)/shard_map/dot_general | solution.py:129
  80.0 0.5 convolution_bitcast_fusion.3
  81.3 0.7 slice_bitcast_fusion.20
  83.2 12.4 %multiply_reduce_fusion.6 = (f32[32,4,128]{2,1,0:T(4,128)S(1)}, f32[32,4,128,128]{3,2,1,0:T(8,128)S(1)}) fusion(f32[32,4,128]{2,1,0:T(4,128)S(1)} %get-tuple-element.7, f32[32,4,128]{2,1,0:T(4,128)S(1)} %get-tuple-element.22, f32[32,4,128,128]{3,2,1,0:T(8,128)} %multiply_add_fusion.3, f32[32,4,128]{2,1,0:T(4,128)S(1)} %get-tuple-element.69, ...), kind=kOutput, calls=%fused_computation.19 | output fusion | flops 16777344 | bytes 17105408 | tf_op jit(solution)/shard_map/mul | solution.py:47
  95.7 9.0 %multiply_reduce_fusion.4 = (f32[32,4,128]{2,1,0:T(4,128)S(1)}, f32[32,4,128,128]{3,2,1,0:T(8,128)}) fusion(f32[32,4,128]{2,1,0:T(4,128)S(1)} %get-tuple-element.10, f32[32,4,128]{2,1,0:T(4,128)S(1)} %get-tuple-element.21, f32[32,4,128,128]{3,2,1,0:T(8,128)S(1)} %get-tuple-element.64, f32[32,4,128]{2,1,0:T(4,128)S(1)} %get-tuple-element.70, ...), kind=kOutput, calls=%fused_computation.15 | output fusion | flops 16777344 | bytes 17105408 | tf_op jit(solution)/shard_map/mul | solution.py:47
  104.7 14.0 %fusion = f32[32,4,128,128]{3,2,1,0:T(8,128)} fusion(f32[32,4,128]{2,1,0:T(4,128)S(1)} %get-tuple-element.72, f32[32,4,128,128]{3,2,1,0:T(8,128)} %get-tuple-element.62, f32[32,4,128]{2,1,0:T(4,128)S(1)} %get-tuple-element.20, f32[32,4,128]{2,1,0:T(4,128)S(1)} %get-tuple-element.12, f32[32,4]{1,0:T(8,128)S(1)} %bitcast.169, ...), kind=kOutput, calls=%fused_computation | output fusion | flops 14713086 | bytes 17039872 | tf_op jit(solution)/shard_map/mul | solution.py:47
  118.7 14.9 %multiply_reduce_fusion.2 = (f32[32,4,128]{2,1,0:T(4,128)S(1)}, f32[32,4,128]{2,1,0:T(4,128)S(1)}) fusion(f32[32,4,128]{2,1,0:T(4,128)} %get-tuple-element.9, f32[32,4,128]{2,1,0:T(4,128)S(1)} %get-tuple-element.19, f32[32,4,128,128]{3,2,1,0:T(8,128)} %fusion, f32[32,4,128]{2,1,0:T(4,128)S(1)} %get-tuple-element.11, f32[32,4]{1,0:T(8,128)S(1)} %bitcast.167, ...), kind=kOutput, calls=%fused_computation.11 | output fusion | flops 31441024 | bytes 17368064 | tf_op jit(solution)/shard_map/mul | solution.py:47
  134.4 33.5 %all_to_all.29 = bf16[16,128,512]{2,1,0:T(8,128)(2,1)S(1)} all-to-all(bf16[16,128,512]{2,1,0:T(8,128)(2,1)S(1)} %broadcast_in_dim.4), channel_id=1, replica_groups=mesh['dp'=4,'kv'=16,'tp'=2] {'kv'}, dimensions={0} | all-to-all | bytes 4194304 | tf_op jit(solution)/shard_map/all_to_all | solution.py:15
  167.9 0.8 convolution_convert_fusion
  168.7 6.1 %all_to_all.30 = bf16[2,2048,64]{1,2,0:T(8,128)(2,1)S(1)} all-to-all(bf16[2,2048,64]{1,2,0:T(8,128)(2,1)S(1)} %bitcast.152), channel_id=1, replica_groups=mesh['dp'=4,'kv'=16,'tp'=2] {'tp'}, dimensions={0} | all-to-all | bytes 1048576 | tf_op jit(solution)/shard_map/all_to_all | solution.py:31
  175.1 12.2 %all_to_all.31 = f32[32,1,2048]{2,1,0:T(1,128)S(1)} all-to-all(f32[32,1,2048]{2,1,0:T(1,128)S(1)} %broadcast_in_dim.5), channel_id=1, replica_groups=mesh['dp'=4,'kv'=16,'tp'=2] {'kv','tp'}, dimensions={0} | all-to-all | bytes 524288 | tf_op jit(solution)/shard_map/all_to_all | solution.py:15
  187.6 0.8 multiply_convert_fusion
  (78 shorter events, 6.9 us)
Async XLA Ops:
  0.6 74.6 %copy-start = (bf16[2048,512]{1,0:T(8,128)(2,1)S(1)}, bf16[2048,512]{1,0:T(8,128)(2,1)}, u32[]{:S(2)}) copy-start(bf16[2048,512]{1,0:T(8,128)(2,1)} %param.23) | copy-start | bytes 6291460
  0.6 64.0 %all-to-all-start = ((bf16[16,128,128]{2,1,0:T(8,128)(2,1)}), bf16[16,128,128]{2,1,0:T(8,128)(2,1)S(1)}, u32[]{:S(2)}, u32[]{:S(2)}) async-start(bf16[16,128,128]{2,1,0:T(8,128)(2,1)} %bitcast.154), calls=%async_computation | async-start | bytes 1048576 | tf_op jit(solution)/shard_map/all_to_all | solution.py:123
  57.5 11.0 %copy-start.8 = (f32[2048]{0:T(1024)S(1)}, f32[2048]{0:T(1024)}, u32[]{:S(2)}) copy-start(f32[2048]{0:T(1024)} %param.19) | copy-start | bytes 24580
  57.5 12.6 %copy-start.10 = (bf16[2048,8]{0,1:T(8,128)(2,1)S(1)}, bf16[2048,8]{0,1:T(8,128)(2,1)}, u32[]{:S(2)}) copy-start(bf16[2048,8]{0,1:T(8,128)(2,1)} %param.25) | copy-start | bytes 98308
  57.5 12.8 %copy-start.11 = (bf16[2048,8]{0,1:T(8,128)(2,1)S(1)}, bf16[2048,8]{0,1:T(8,128)(2,1)}, u32[]{:S(2)}) copy-start(bf16[2048,8]{0,1:T(8,128)(2,1)} %param.24) | copy-start | bytes 98308
  75.2 4.8 %copy-start.2 = (bf16[2048,512]{1,0:T(8,128)(2,1)S(1)}, bf16[2048,512]{1,0:T(8,128)(2,1)}, u32[]{:S(2)}) copy-start(bf16[2048,512]{1,0:T(8,128)(2,1)} %param.20) | copy-start | bytes 6291460
  77.9 5.3 %copy-start.7 = (f32[32,1,4]{2,0,1:T(8,128)S(1)}, f32[32,1,4]{2,0,1:T(8,128)}, u32[]{:S(2)}) copy-start(f32[32,1,4]{2,0,1:T(8,128)} %copy.113) | copy-start | bytes 1540
  83.2 21.5 %copy-start.4 = (f32[32,4,128]{2,1,0:T(4,128)}, f32[32,4,128]{2,1,0:T(4,128)S(1)}, u32[]{:S(2)}) copy-start(f32[32,4,128]{2,1,0:T(4,128)S(1)} %get-tuple-element.12) | copy-start | bytes 196612
  83.2 12.5 %copy-start.6 = (f32[32,1,4]{2,0,1:T(8,128)S(1)}, f32[32,1,4]{2,0,1:T(8,128)}, u32[]{:S(2)}) copy-start(f32[32,1,4]{2,0,1:T(8,128)} %copy.115) | copy-start | bytes 1540
  95.7 9.0 %copy-start.5 = (f32[32,1,4]{2,0,1:T(8,128)S(1)}, f32[32,1,4]{2,0,1:T(8,128)}, u32[]{:S(2)}) copy-start(f32[32,1,4]{2,0,1:T(8,128)} %copy.117) | copy-start | bytes 1540
  118.7 15.4 %copy-start.9 = (f32[512]{0:T(512)S(1)}, f32[512]{0:T(512)}, u32[]{:S(2)}) copy-start(f32[512]{0:T(512)} %broadcast_bitcast_fusion) | copy-start | bytes 6148
  118.7 49.2 %copy-start.3 = (bf16[512,128]{1,0:T(8,128)(2,1)S(1)}, bf16[512,128]{1,0:T(8,128)(2,1)}, u32[]{:S(2)}) copy-start(bf16[512,128]{1,0:T(8,128)(2,1)} %param.28) | copy-start | bytes 393220
  118.7 69.6 %copy-start.1 = (bf16[2048,512]{1,0:T(8,128)(2,1)S(1)}, bf16[2048,512]{1,0:T(8,128)(2,1)}, u32[]{:S(2)}) copy-start(bf16[2048,512]{1,0:T(8,128)(2,1)} %param.23) | copy-start | bytes 6291460
  133.6 54.0 %copy-start.12 = (f32[64]{0:T(128)S(1)}, f32[64]{0:T(128)}, u32[]{:S(2)}) copy-start(f32[64]{0:T(128)} %param.29) | copy-start | bytes 772
where the time goes:
time: 189 us; the launch traced here: 188 us
  other arithmetic  110 us (58%)
  blocking collectives  51.8 us (27%)
  local copies, waits for them, and re-layouts  10.8 us (6%)
  starting transfers between devices  8.73 us (5%)
  matrix products  6.39 us (3%)
    mul x10, other arithmetic, advance(): rate_cube * key_row[..., :, None] * recalled[..., None, :]  98.3 us
    all_to_all x2, blocking collectives, from_everyone(): lax.all_to_all(jnp.broadcast_to(shard[None], (count, *shard.shape)), axis...  45.7 us
    all_to_all x1, starting transfers between devices, local(): lax.all_to_all(tokens, 'kv', split_axis=0, concat_axis=1, tiled=True)  8.73 us
    all_to_all x1, blocking collectives, summed_on_arrival(): tiles = lax.all_to_all(cut_along(shard, dim, count), axis, 0, 0, tiled=True)  6.1 us
    dot_general x4, matrix products, local(): jnp.dot(scaled, weight, preferred_element_type=jnp.float32)  5.21 us
  transfers between devices with their start and end apart: 1, of which 0 were waited for; matrix products, arithmetic and copies ran while one was open for 29% of the time, Pallas kernels for 0%

commit v1 on v0

v1 whole, which is shorter than its diff:
```python
import functools

import jax
import jax.numpy as jnp
from jax import lax
from jax.experimental import pallas as pl
from jax.experimental.pallas import tpu as pltpu
from jax.sharding import PartitionSpec as P

MESH = pl.DeviceIdType.MESH
F32 = jnp.float32
BF16 = jnp.bfloat16
HIGH = lax.Precision.HIGHEST
VM = pltpu.VMEM
NT = (((1,), (1,)), ((), ()))
TN = (((0,), (0,)), ((), ()))


def mm(a, b):
    return jnp.dot(a, b, preferred_element_type=F32)


def mm_nt(a, b):
    return lax.dot_general(a, b, NT, preferred_element_type=F32)


def silu(v):
    return v / (1.0 + jnp.exp(-v))


def unit(v):
    return v * lax.rsqrt(jnp.sum(v * v, axis=-1, keepdims=True) + 1e-06)


def quad_rows(wide, rows):
    own = lax.broadcasted_iota(jnp.int32, (rows, 128), 0) % 16 // 4
    out = wide[:, 0:128]
    for q in range(1, 4):
        out = jnp.where(own == q, wide[:, 128 * q : 128 * q + 128], out)
    return out


def masks():
    r = lax.broadcasted_iota(jnp.int32, (128, 128), 0)
    c = lax.broadcasted_iota(jnp.int32, (128, 128), 1)
    same = r // 4 == c // 4
    return r == c, same & (c < r), same & (c <= r)


def as_row(col, eye):
    return jnp.sum(jnp.where(eye, col, 0.0), axis=0, keepdims=True)


def ratios(c_col, c_row, keep):
    return jnp.where(keep, jnp.exp(jnp.where(keep, c_col - c_row, 0.0)), 0.0)


def nilpotent(a):
    ab = a.astype(BF16)
    square = mm(ab, ab)
    return square - a - mm(ab, square.astype(BF16))


def main_kernel(
    n,
    tokens, pre_gain, wq, wk, wv, wg, beta_t, decay_t, decay_log, head_gain, out_w, saved,
    ekeys, evals, erates, edecays, accepted,
    state, mixed_in,
    tok, x, w, ow, wt, state_b, ek, ev, k1b, r1, rq, k2b, q2b, v2, gates, tot, proj, scal, ssq, att,
    part, psend, precv, msend,
    tok_sem, ow_sem, s_sem, w_sem, tsend, trecv, gsend, grecv, xsend, xrecv, osend, orecv,
):
    me = lax.axis_index("kv")
    core = lax.axis_index("tp")
    width = n * 128

    load_tok = pltpu.make_async_copy(tokens, tok, tok_sem)
    load_ow = pltpu.make_async_copy(out_w, ow, ow_sem)
    load_tok.start()
    load_ow.start()
    load_s = [pltpu.make_async_copy(saved.at[pl.ds(4 * t, 4)], state.at[pl.ds(4 * t, 4)], s_sem.at[t]) for t in range(8)]
    for c in load_s:
        c.start()
    load_w = [pltpu.make_async_copy(src, w.at[i], w_sem.at[i]) for i, src in enumerate((wq, wk, wv, wg))]
    for c in load_w:
        c.start()

    barrier = pltpu.get_barrier_semaphore()
    for d in range(1, n):
        pl.semaphore_signal(barrier, inc=1, device_id={"kv": lax.rem(me + d, n), "tp": core}, device_id_type=MESH)
    pl.semaphore_signal(barrier, inc=1, device_id={"kv": me, "tp": 1 - core}, device_id_type=MESH)

    eye, strict, incl = masks()
    load_ow.wait()
    wt[pl.ds(me, 1)] = mm_nt(jnp.where(eye, 1.0, 0.0).astype(BF16), ow[...]).astype(BF16)[None]
    load_tok.wait()
    x[pl.ds(me, 1)] = tok[pl.ds(pl.multiple_of(me * 128, 128), 128), :][None]

    pl.semaphore_wait(barrier, n)

    def to_peer(src, dst, ssem, rsem, peer):
        return pltpu.make_async_remote_copy(
            src_ref=src, dst_ref=dst, send_sem=ssem, recv_sem=rsem,
            device_id={"kv": peer, "tp": core}, device_id_type=MESH,
        )

    def send_tok(d):
        peer = lax.rem(me + d, n)
        rows = pl.ds(pl.multiple_of(peer * 128, 128), 128)
        return to_peer(tok.at[rows, :], x.at[me], tsend.at[d], trecv.at[me], peer)

    def send_wt(d):
        peer = lax.rem(me + d, n)
        return to_peer(wt.at[me], wt.at[me], gsend.at[d], grecv.at[me], peer)

    for d in range(1, n):
        send_tok(d).start()
    for d in range(1, n):
        send_wt(d).start()

    keys = unit(ekeys[...].astype(F32))
    ek[...] = keys
    ev[...] = evals[...].astype(F32)
    count = accepted[...]
    total = jnp.zeros((4, 32), F32)
    rate_p, cum_p = [], []
    for p in range(4):
        live = jnp.where(p < count, 1.0, 0.0)
        total = total + edecays[p] * live
        rate_p.append(erates[p] * live)
        cum_p.append(total)
    row = lax.broadcasted_iota(jnp.int32, (128, 32), 0)
    seq = lax.broadcasted_iota(jnp.int32, (128, 32), 1)

    def expand(pieces):
        out = jnp.zeros((128, 4), F32)
        for p in range(4):
            pick = jnp.where(row == 4 * seq + p, 1.0, 0.0)
            out = out + lax.dot_general(pick, pieces[p], NT, precision=HIGH, preferred_element_type=F32)
        return out

    rate1 = expand(rate_p)
    cum1 = expand(cum_p)
    tot1 = expand([total] * 4)
    for h in range(4):
        k1b[h] = ek[pl.ds(h, 128, stride=4), :].astype(BF16)
        tot[h] = jnp.broadcast_to(jnp.exp(tot1[:, h : h + 1]), (128, 128))
    for c in load_s:
        c.wait()

    def recall(t, _):
        rows = pl.ds(pl.multiple_of(16 * t, 16), 16)
        for h in range(4):
            wide = jnp.concatenate([state[4 * t + q, h].astype(BF16) for q in range(4)], axis=1)
            r1[h, rows, :] = quad_rows(mm(k1b[h, rows, :], wide), 16)
        return 0

    lax.fori_loop(0, 8, recall, 0)

    for h in range(4):
        b = rate1[:, h : h + 1]
        c_col = cum1[:, h : h + 1]
        kb = k1b[h]
        a = b * ratios(c_col, as_row(c_col, eye), strict) * mm_nt(kb, kb)
        rhs = b * (ev[pl.ds(h, 128, stride=4), :] - jnp.exp(c_col) * r1[h])
        u = rhs + mm(nilpotent(a).astype(BF16), rhs.astype(BF16))
        r1[h] = u * jnp.exp(tot1[:, h : h + 1] - c_col)

    own = lax.broadcasted_iota(jnp.int32, (16, 128), 0) // 4

    def fold(t, _):
        rows = pl.ds(pl.multiple_of(16 * t, 16), 16)
        for h in range(4):
            u = r1[h, rows, :]
            wide = jnp.concatenate([jnp.where(own == q, u, 0.0) for q in range(4)], axis=1).astype(BF16)
            step = lax.dot_general(k1b[h, rows, :], wide, TN, preferred_element_type=F32)
            for q in range(4):
                new = state[4 * t + q, h] * tot[h, pl.ds(16 * t + 4 * q, 1), :] + step[:, 128 * q : 128 * q + 128]
                state[4 * t + q, h] = new
                state_b[h, t, :, 128 * q : 128 * q + 128] = new.astype(BF16)
        return 0

    lax.fori_loop(0, 8, fold, 0)

    for c in load_w:
        c.wait()
    proj[...] = jnp.zeros_like(proj)
    scal[...] = jnp.zeros_like(scal)
    ssq[...] = jnp.zeros_like(ssq)
    for g in range(n // 4):
        group = lax.rem(me // 4 + g, n // 4)
        for i in range(4):
            src = 4 * group + i

            @pl.when(src != me)
            def _():
                to_peer(tok.at[pl.ds(0, 128), :], x.at[src], tsend.at[0], trecv.at[src], src).wait_recv()

        pieces = []
        square = jnp.zeros((128, 128), F32)
        for i in range(4):
            wide = x[pl.ds(4 * group + i, 1)][0].astype(F32)
            square = square + wide * wide
            pieces.append((wide * pre_gain[pl.ds(4 * group + i, 1), :]).astype(BF16))
        scaled = jnp.concatenate(pieces, axis=1)
        ssq[...] += square
        cols = pl.ds(pl.multiple_of(group * 512, 512), 512)
        scal[0] += mm_nt(scaled, beta_t[:, cols])
        scal[1] += mm_nt(scaled, decay_t[:, cols])
        for i in range(4):
            proj[i] += mm(scaled, w[i, cols, :])
    inverse = lax.rsqrt(jnp.sum(ssq[...], axis=1, keepdims=True) / width + 1e-06)
    beta_raw = scal[0] * inverse
    decay_raw = scal[1] * inverse
    rates8 = 1.0 / (1.0 + jnp.exp(-beta_raw))
    soft8 = jnp.maximum(decay_raw, 0.0) + jnp.log1p(jnp.exp(-jnp.abs(decay_raw)))
    for h in range(4):
        lanes = slice(128 * h, 128 * h + 128)
        q2b[h] = (unit(silu(proj[0, :, lanes] * inverse)) * 128 ** (-0.5)).astype(BF16)
        k2b[h] = unit(silu(proj[1, :, lanes] * inverse)).astype(BF16)
        v2[h] = silu(proj[2, :, lanes] * inverse)
        gates[h] = silu(proj[3, :, lanes] * inverse) * head_gain[...]

    def recall_new(t, _):
        rows = pl.ds(pl.multiple_of(16 * t, 16), 16)
        for h in range(4):
            both = jnp.concatenate([k2b[h, rows, :], q2b[h, rows, :]], axis=0)
            out = quad_rows(mm(both, state_b[h, t]), 32)
            r1[h, rows, :] = out[:16]
            rq[h, rows, :] = out[16:]
        return 0

    lax.fori_loop(0, 8, recall_new, 0)

    upper = core > 0
    pos = lax.broadcasted_iota(jnp.int32, (128, 1), 0) % 4
    for h in range(4):
        b = jnp.where(upper, rates8[:, h + 4 : h + 5], rates8[:, h : h + 1])
        g = jnp.where(upper, soft8[:, h + 4 : h + 5], soft8[:, h : h + 1])
        g = -jnp.exp(jnp.full((1, 1), decay_log[0, h], F32)) * g
        c_col = jnp.sum(jnp.where(incl, as_row(g, eye), 0.0), axis=1, keepdims=True)
        ratio = ratios(c_col, as_row(c_col, eye), incl)
        kb = k2b[h]
        a = jnp.where(strict, b * ratio * mm_nt(kb, kb), 0.0)
        seen = ratio * mm_nt(q2b[h], kb)
        seen = seen + mm(seen.astype(BF16), nilpotent(a).astype(BF16))
        grown = jnp.exp(c_col)
        rhs = b * (v2[h] - grown * r1[h])
        reads = grown * rq[h] + mm(seen.astype(BF16), rhs.astype(BF16))
        normed = reads * lax.rsqrt(jnp.mean(reads * reads, axis=-1, keepdims=True) + 1e-06)
        att[:, 128 * h : 128 * h + 128] = (normed * gates[h]).astype(BF16)

    for d in range(1, n):
        src = lax.rem(me + d, n)
        to_peer(wt.at[me], wt.at[src], gsend.at[0], grecv.at[src], src).wait_recv()
    per = n // 4

    def swap(c):
        rows = pl.ds(c * per, per)
        return pltpu.make_async_remote_copy(
            src_ref=psend.at[rows], dst_ref=precv.at[rows], send_sem=xsend.at[c], recv_sem=xrecv.at[c],
            device_id={"kv": me, "tp": 1 - core}, device_id_type=MESH,
        )

    attended = att[...]
    for c in range(4):
        for i in range(c * per, c * per + per):
            out = mm_nt(wt[i], attended)
            part[i] = out
            psend[i] = out.astype(BF16)
        swap(c).start()
    squares = jnp.zeros((128, 128), F32)
    for c in range(4):
        swap(c).wait_recv()
        for i in range(c * per, c * per + per):
            both = part[i] + precv[i].astype(F32)
            squares = squares + both * both
    factor = lax.rsqrt(jnp.sum(squares, axis=0, keepdims=True) / width + 1e-06)
    half = pl.ds(pl.multiple_of(core * 64, 64), 64)
    for i in range(n):
        both = part[i, half, :] + precv[i, half, :].astype(F32)
        msend[i] = (both * factor).astype(BF16)
    mixed_in[pl.ds(me, 1)] = msend[pl.ds(me, 1)]

    def send_out(d):
        peer = lax.rem(me + d, n)
        return to_peer(msend.at[peer], mixed_in.at[me], osend.at[d], orecv.at[me], peer)

    for d in range(1, n):
        send_out(d).start()
    for d in range(1, n):
        src = lax.rem(me + d, n)
        to_peer(msend.at[me], mixed_in.at[src], osend.at[0], orecv.at[src], src).wait_recv()
    for d in range(1, n):
        send_tok(d).wait_send()
        send_wt(d).wait_send()
        send_out(d).wait_send()
    for c in range(4):
        swap(c).wait_send()


def last_kernel(n, state, mixed_in, post_gain, committed, mixed, sem):
    copies = [pltpu.make_async_copy(state.at[pl.ds(8 * t, 8)], committed.at[pl.ds(8 * t, 8)], sem.at[t]) for t in range(4)]
    for c in copies:
        c.start()
    i = lax.broadcasted_iota(jnp.int32, (64, 64), 0)
    j = lax.broadcasted_iota(jnp.int32, (64, 64), 1)
    gain = jnp.sum(jnp.where(i == j, post_gain[...], 0.0), axis=1, keepdims=True)
    for k in range(n):
        mixed[:, 128 * k : 128 * k + 128] = (mixed_in[k].astype(F32) * gain).astype(BF16)
    for c in copies:
        c.wait()


def local(
    n,
    tokens, pre_gain, query_weight, key_weight, value_weight, gate_weight, beta_weight, decay_weight, decay_log,
    head_gain, out_weight, post_gain, saved_state, earlier_keys, earlier_values, earlier_rates, earlier_decays, accepted,
):
    any_spec = pl.BlockSpec(memory_space=pl.ANY)
    vmem = pl.BlockSpec(memory_space=VM)
    smem = pl.BlockSpec(memory_space=pltpu.SMEM)
    dma = pltpu.SemaphoreType.DMA
    heads = (4, 128, 128)
    state, mixed_in = pl.pallas_call(
        functools.partial(main_kernel, n),
        out_shape=(VM(saved_state.shape, F32), VM((n, 64, 128), BF16)),
        in_specs=[any_spec, vmem, any_spec, any_spec, any_spec, any_spec, vmem, vmem, smem, vmem, any_spec, any_spec]
        + [vmem] * 5,
        out_specs=(vmem, vmem),
        scratch_shapes=[
            VM((n * 128, 128), BF16),
            VM((n, 128, 128), BF16),
            VM((4, n * 128, 512), BF16),
            VM((512, 128), BF16),
            VM((n, 128, 512), BF16),
            VM((4, 8, 128, 512), BF16),
            VM((512, 128), F32),
            VM((512, 128), F32),
            VM(heads, BF16),
            VM(heads, F32),
            VM(heads, F32),
            VM(heads, BF16),
            VM(heads, BF16),
            VM(heads, F32),
            VM(heads, F32),
            VM(heads, F32),
            VM((4, 128, 512), F32),
            VM((2, 128, 8), F32),
            VM((128, 128), F32),
            VM((128, 512), BF16),
            VM((n, 128, 128), F32),
            VM((n, 128, 128), BF16),
            VM((n, 128, 128), BF16),
            VM((n, 64, 128), BF16),
            dma, dma, dma((8,)), dma((4,)), dma((n,)), dma((n,)), dma((n,)), dma((n,)), dma((4,)), dma((4,)), dma((n,)), dma((n,)),
        ],
        compiler_params=pltpu.CompilerParams(collective_id=0, has_side_effects=True, vmem_limit_bytes=48 << 20),
        name="delta_step",
    )(
        tokens, pre_gain.reshape(n, 128), query_weight, key_weight, value_weight, gate_weight, beta_weight.T,
        decay_weight.T, decay_log.reshape(1, 4), head_gain.reshape(1, 128), out_weight, saved_state,
        earlier_keys.reshape(512, 128), earlier_values.reshape(512, 128), earlier_rates.transpose(1, 2, 0),
        earlier_decays.transpose(1, 2, 0), accepted.reshape(1, 32),
    )
    committed, mixed = pl.pallas_call(
        functools.partial(last_kernel, n),
        out_shape=(jax.ShapeDtypeStruct(saved_state.shape, F32), jax.ShapeDtypeStruct((64, n * 128), BF16)),
        in_specs=[vmem] * 3,
        out_specs=(any_spec, vmem),
        scratch_shapes=[dma((4,))],
        compiler_params=pltpu.CompilerParams(vmem_limit_bytes=16 << 20),
        name="write_out",
    )(state, mixed_in, post_gain.reshape(1, 64))
    return mixed.T, committed


def solution(mesh):
    placed = (
        P("dp", "kv"), P(), P(None, "tp"), P(None, "tp"), P(None, "tp"), P(None, "tp"), P(), P(), P("tp"), P(),
        P("tp", "kv"), P(("kv", "tp")), P(("dp", "kv"), "tp", None, None), P(("dp", "kv"), None, "tp", None),
        P(("dp", "kv"), None, "tp", None), P(("dp", "kv"), None, "tp"), P(("dp", "kv"), None, "tp"), P(("dp", "kv")),
    )
    return jax.shard_map(
        functools.partial(local, mesh.shape["kv"]),
        mesh=mesh,
        in_specs=placed,
        out_specs=(P("dp", ("kv", "tp")), P(("dp", "kv"), "tp", None, None)),
        check_vma=False,
    )
```

time: 189 us -> 59.8 us (0.32)
  other arithmetic: 110 us -> 0 us
  Pallas kernels: 0 us -> 59 us
  blocking collectives: 51.8 us -> 0 us
  local copies, waits for them, and re-layouts: 10.8 us -> 0.01 us
  starting transfers between devices: 8.73 us -> 0 us
  matrix products: 6.39 us -> 0 us
    mul x19 -> x0, other arithmetic: 101 us -> none  [the longest x10 98.3 us: advance(): rate_cube * key_row[..., :, None] * recalled[..., None, :]]
    pallas_call x0 -> x2, Pallas kernels: none -> 59 us  [the longest x1 55 us: local(): pl.pallas_call(functools.partial(main_kernel, n), out_shape=(VM(saved_sta...]
    all_to_all x3 -> x0, blocking collectives: 51.8 us -> none  [the longest x2 45.7 us: from_everyone(): lax.all_to_all(jnp.broadcast_to(shard[None], (count, *shard.shape)), axis...]
    all_to_all x1 -> x0, starting transfers between devices: 8.73 us -> none  [local(): lax.all_to_all(tokens, 'kv', split_axis=0, concat_axis=1, tiled=True)]
    dot_general x7 -> x0, matrix products: 6.39 us -> none  [the longest x4 5.21 us: local(): jnp.dot(scaled, weight, preferred_element_type=jnp.float32)]
    convert_element_type x6 -> x0, other arithmetic: 5.13 us -> none  [the longest x1 1.56 us: local(): scaled = (widened * pre_gain).astype(jnp.bfloat16)]
    mul x12 -> x0, local copies, waits for them, and re-layouts: 3.68 us -> none  [the longest x1 1.24 us: local(): reads * lax.rsqrt(jnp.mean(reads * reads, axis=-1, keepdims=True) + 1e-06)]
    exp x9 -> x0, local copies, waits for them, and re-layouts: 3.45 us -> none  [advance(): jnp.exp(log_decay)[..., None, None] * current]
  transfers between devices with their start and end apart: 1 -> 0, of which waited for: 0 -> 0; matrix products, arithmetic and copies ran while one was open for 29% -> 0% of each run, Pallas kernels for 0% -> 0%
where the time goes in v1:
time: 59.8 us; the launch traced here: 59.7 us
  Pallas kernels  59 us (99%)
  between operations  0.66 us (1%)
    pallas_call x1, Pallas kernels, local(): pl.pallas_call(functools.partial(main_kernel, n), out_shape=(VM(saved_sta...  55 us
    pallas_call x1, Pallas kernels, local(): pl.pallas_call(functools.partial(last_kernel, n), out_shape=(jax.ShapeDty...  4.07 us

profile of v1, /device:TPU:1, one launch (start us, length us, event | category | flops | bytes accessed | tf_op | source)
XLA Modules:
  0.0 59.7 jit_solution(3568530061174120123)
XLA Ops:
  0.6 0.0 copy-start
  0.6 55.0 %delta_step.1 = (f32[32,4,128,128]{3,2,1,0:T(8,128)S(1)}, bf16[16,64,128]{2,1,0:T(8,128)(2,1)S(1)}) custom-call(bf16[2048,128]{1,0:T(8,128)(2,1)} %tokens.1, f32[16,128]{1,0:T(8,128)} %bitcast.17, bf16[2048,512]{1,0:T(8,128)(2,1)} %wq.1, bf16[2048,512]{1,0:T(8,128)(2,1)} %wk.1, bf16[2048,512]{1,0:T(8,128)(2,1)} %wv.1, bf16[2048,512]{1,0:T(8,128)(2,1)} %wg.1, ...), custom_call_target="tpu_custom_call" | custom-call | tf_op jit(solution)/shard_map/delta_step/pallas_call | solution.py:325
  55.6 0.0 copy-done
  55.6 4.1 %write_out.1 = (f32[32,4,128,128]{3,2,1,0:T(8,128)}, bf16[64,2048]{1,0:T(8,128)(2,1)}) custom-call(f32[32,4,128,128]{3,2,1,0:T(8,128)S(1)} %get-tuple-element.6.state, bf16[16,64,128]{2,1,0:T(8,128)(2,1)S(1)} %get-tuple-element.7.mixed_in, f32[1,64]{1,0:T(1,128)S(1)} %bitcast.12), custom_call_target="tpu_custom_call" | custom-call | tf_op jit(solution)/shard_map/write_out/pallas_call | solution.py:366
Async XLA Ops:
  0.6 55.0 %copy-start = (f32[64]{0:T(128)S(1)}, f32[64]{0:T(128)}, u32[]{:S(2)}) copy-start(f32[64]{0:T(128)} %param.29) | copy-start | bytes 772

commit v2 on v1

--- a/solution.py
+++ b/solution.py
@@ -109,14 +109,62 @@
         rows = pl.ds(pl.multiple_of(peer * 128, 128), 128)
         return to_peer(tok.at[rows, :], x.at[me], tsend.at[d], trecv.at[me], peer)
 
-    def send_wt(d):
-        peer = lax.rem(me + d, n)
-        return to_peer(wt.at[me], wt.at[me], gsend.at[d], grecv.at[me], peer)
+    step_a, step_b = 1 + 3 * core, 4 - 3 * core
+    at_a, at_b = lax.rem(me // step_a, 4), lax.rem(me // step_b, 4)
+
+    def place(da, db):
+        return lax.rem(at_a + da + 4, 4) * step_a + lax.rem(at_b + db + 4, 4) * step_b
+
+    sent = []
+
+    def part_of(block, side):
+        return wt.at[block] if side is None else wt.at[block, pl.ds(64 * side, 64)]
+
+    def pass_on(block, side, peer):
+        copy = to_peer(
+            part_of(block, side), part_of(block, side), gsend.at[len(sent)], grecv.at[block, 1 if side == 1 else 0], peer
+        )
+        copy.start()
+        sent.append(copy)
+
+    def arrived(block, side):
+        to_peer(part_of(block, side), part_of(block, side), gsend.at[0], grecv.at[block, 1 if side == 1 else 0], me).wait_recv()
+
+    def to_b(da):
+        for db in (1, -1):
+            pass_on(place(da, 0), None, place(0, db))
+
+    def relay_b(da):
+        for db in (1, -1):
+            arrived(place(da, db), None)
+            pass_on(place(da, db), 1 if db == 1 else 0, place(0, -db))
+
+    def gather_first():
+        for da in (1, -1):
+            pass_on(me, None, place(da, 0))
+        to_b(0)
+
+    def gather_second():
+        for da in (1, -1):
+            arrived(place(da, 0), None)
+            pass_on(place(da, 0), 1 if da == 1 else 0, place(-da, 0))
+        to_b(1)
+        to_b(-1)
+
+    def gather_third():
+        for side in (0, 1):
+            arrived(place(2, 0), side)
+        to_b(2)
+        relay_b(0)
+
+    def gather_last():
+        for da in range(4):
+            for side in (0, 1):
+                arrived(place(da, 2), side)
 
     for d in range(1, n):
         send_tok(d).start()
-    for d in range(1, n):
-        send_wt(d).start()
+    gather_first()
 
     keys = unit(ekeys[...].astype(F32))
     ek[...] = keys
@@ -156,6 +204,7 @@
         return 0
 
     lax.fori_loop(0, 8, recall, 0)
+    gather_second()
 
     for h in range(4):
         b = rate1[:, h : h + 1]
@@ -166,6 +215,7 @@
         u = rhs + mm(nilpotent(a).astype(BF16), rhs.astype(BF16))
         r1[h] = u * jnp.exp(tot1[:, h : h + 1] - c_col)
 
+    gather_third()
     own = lax.broadcasted_iota(jnp.int32, (16, 128), 0) // 4
 
     def fold(t, _):
@@ -181,6 +231,8 @@
         return 0
 
     lax.fori_loop(0, 8, fold, 0)
+    relay_b(1)
+    relay_b(-1)
 
     for c in load_w:
         c.wait()
@@ -209,6 +261,7 @@
         scal[1] += mm_nt(scaled, decay_t[:, cols])
         for i in range(4):
             proj[i] += mm(scaled, w[i, cols, :])
+    relay_b(2)
     inverse = lax.rsqrt(jnp.sum(ssq[...], axis=1, keepdims=True) / width + 1e-06)
     beta_raw = scal[0] * inverse
     decay_raw = scal[1] * inverse
@@ -250,9 +303,7 @@
         normed = reads * lax.rsqrt(jnp.mean(reads * reads, axis=-1, keepdims=True) + 1e-06)
         att[:, 128 * h : 128 * h + 128] = (normed * gates[h]).astype(BF16)
 
-    for d in range(1, n):
-        src = lax.rem(me + d, n)
-        to_peer(wt.at[me], wt.at[src], gsend.at[0], grecv.at[src], src).wait_recv()
+    gather_last()
     per = n // 4
 
     def swap(c):
@@ -293,10 +344,11 @@
         to_peer(msend.at[me], mixed_in.at[src], osend.at[0], orecv.at[src], src).wait_recv()
     for d in range(1, n):
         send_tok(d).wait_send()
-        send_wt(d).wait_send()
         send_out(d).wait_send()
     for c in range(4):
         swap(c).wait_send()
+    for copy in sent:
+        copy.wait_send()
 
 
 def last_kernel(n, state, mixed_in, post_gain, committed, mixed, sem):
@@ -353,7 +405,7 @@
             VM((n, 128, 128), BF16),
             VM((n, 128, 128), BF16),
             VM((n, 64, 128), BF16),
-            dma, dma, dma((8,)), dma((4,)), dma((n,)), dma((n,)), dma((n,)), dma((n,)), dma((4,)), dma((4,)), dma((n,)), dma((n,)),
+            dma, dma, dma((8,)), dma((4,)), dma((n,)), dma((n,)), dma((20,)), dma((n, 2)), dma((4,)), dma((4,)), dma((n,)), dma((n,)),
         ],
         compiler_params=pltpu.CompilerParams(collective_id=0, has_side_effects=True, vmem_limit_bytes=48 << 20),
         name="delta_step",

time: 59.8 us -> 47.9 us (0.80)
  Pallas kernels: 59 us -> 47.1 us
    pallas_call x1, Pallas kernels: 55 us -> 43 us  [local(): pl.pallas_call(functools.partial(main_kernel, n), out_shape=(VM(saved_sta...]
where the time goes in v2:
time: 47.9 us; the launch traced here: 47.7 us
  Pallas kernels  47.1 us (98%)
  between operations  0.66 us (1%)
    pallas_call x1, Pallas kernels, local(): pl.pallas_call(functools.partial(main_kernel, n), out_shape=(VM(saved_sta...  43 us
    pallas_call x1, Pallas kernels, local(): pl.pallas_call(functools.partial(last_kernel, n), out_shape=(jax.ShapeDty...  4.07 us

profile of v2, /device:TPU:1, one launch (start us, length us, event | category | flops | bytes accessed | tf_op | source)
XLA Modules:
  0.0 47.7 jit_solution(14062984501392490812)
XLA Ops:
  0.6 0.0 copy-start
  0.6 43.0 %delta_step.1 = (f32[32,4,128,128]{3,2,1,0:T(8,128)S(1)}, bf16[16,64,128]{2,1,0:T(8,128)(2,1)S(1)}) custom-call(bf16[2048,128]{1,0:T(8,128)(2,1)} %tokens.1, f32[16,128]{1,0:T(8,128)} %bitcast.17, bf16[2048,512]{1,0:T(8,128)(2,1)} %wq.1, bf16[2048,512]{1,0:T(8,128)(2,1)} %wk.1, bf16[2048,512]{1,0:T(8,128)(2,1)} %wv.1, bf16[2048,512]{1,0:T(8,128)(2,1)} %wg.1, ...), custom_call_target="tpu_custom_call" | custom-call | tf_op jit(solution)/shard_map/delta_step/pallas_call | solution.py:377
  43.7 0.0 copy-done
  43.7 4.1 %write_out.1 = (f32[32,4,128,128]{3,2,1,0:T(8,128)}, bf16[64,2048]{1,0:T(8,128)(2,1)}) custom-call(f32[32,4,128,128]{3,2,1,0:T(8,128)S(1)} %get-tuple-element.6.state, bf16[16,64,128]{2,1,0:T(8,128)(2,1)S(1)} %get-tuple-element.7.mixed_in, f32[1,64]{1,0:T(1,128)S(1)} %bitcast.12), custom_call_target="tpu_custom_call" | custom-call | tf_op jit(solution)/shard_map/write_out/pallas_call | solution.py:418
Async XLA Ops:
  0.6 43.0 %copy-start = (f32[64]{0:T(128)S(1)}, f32[64]{0:T(128)}, u32[]{:S(2)}) copy-start(f32[64]{0:T(128)} %param.29) | copy-start | bytes 772

commit v3 on v2

--- a/solution.py
+++ b/solution.py
@@ -68,7 +68,7 @@
     state, mixed_in,
     tok, x, w, ow, wt, state_b, ek, ev, k1b, r1, rq, k2b, q2b, v2, gates, tot, proj, scal, ssq, att,
     part, psend, precv, msend,
-    tok_sem, ow_sem, s_sem, w_sem, tsend, trecv, gsend, grecv, xsend, xrecv, osend, orecv,
+    tok_sem, ow_sem, s_sem, w_sem, tsend, trecv, gsend, grecv, xsend, xrecv, osend, orecv, fsend, frecv,
 ):
     me = lax.axis_index("kv")
     core = lax.axis_index("tp")
@@ -78,23 +78,23 @@
     load_ow = pltpu.make_async_copy(out_w, ow, ow_sem)
     load_tok.start()
     load_ow.start()
+    barrier = pltpu.get_barrier_semaphore()
+    for d in range(1, n):
+        pl.semaphore_signal(barrier, inc=1, device_id={"kv": lax.rem(me + d, n), "tp": core}, device_id_type=MESH)
+    pl.semaphore_signal(barrier, inc=1, device_id={"kv": me, "tp": 1 - core}, device_id_type=MESH)
+
+    eye, strict, incl = masks()
+    load_tok.wait()
+    load_ow.wait()
     load_s = [pltpu.make_async_copy(saved.at[pl.ds(4 * t, 4)], state.at[pl.ds(4 * t, 4)], s_sem.at[t]) for t in range(8)]
     for c in load_s:
         c.start()
     load_w = [pltpu.make_async_copy(src, w.at[i], w_sem.at[i]) for i, src in enumerate((wq, wk, wv, wg))]
     for c in load_w:
         c.start()
-
-    barrier = pltpu.get_barrier_semaphore()
-    for d in range(1, n):
-        pl.semaphore_signal(barrier, inc=1, device_id={"kv": lax.rem(me + d, n), "tp": core}, device_id_type=MESH)
-    pl.semaphore_signal(barrier, inc=1, device_id={"kv": me, "tp": 1 - core}, device_id_type=MESH)
-
-    eye, strict, incl = masks()
-    load_ow.wait()
     wt[pl.ds(me, 1)] = mm_nt(jnp.where(eye, 1.0, 0.0).astype(BF16), ow[...]).astype(BF16)[None]
-    load_tok.wait()
-    x[pl.ds(me, 1)] = tok[pl.ds(pl.multiple_of(me * 128, 128), 128), :][None]
+    half = pl.ds(pl.multiple_of(core * 64, 64), 64)
+    x[pl.ds(me, 1), half, :] = tok[pl.ds(pl.multiple_of(me * 128 + core * 64, 64), 64), :][None]
 
     pl.semaphore_wait(barrier, n)
 
@@ -106,8 +106,15 @@
 
     def send_tok(d):
         peer = lax.rem(me + d, n)
-        rows = pl.ds(pl.multiple_of(peer * 128, 128), 128)
-        return to_peer(tok.at[rows, :], x.at[me], tsend.at[d], trecv.at[me], peer)
+        rows = pl.ds(pl.multiple_of(peer * 128 + core * 64, 64), 64)
+        return to_peer(tok.at[rows, :], x.at[me, half, :], tsend.at[d], trecv.at[me], peer)
+
+    def share(g):
+        some = x.at[pl.ds(4 * lax.rem(me // 4 + g, n // 4), 4), half, :]
+        return pltpu.make_async_remote_copy(
+            src_ref=some, dst_ref=some, send_sem=fsend.at[g], recv_sem=frecv.at[g],
+            device_id={"kv": me, "tp": 1 - core}, device_id_type=MESH,
+        )
 
     step_a, step_b = 1 + 3 * core, 4 - 3 * core
     at_a, at_b = lax.rem(me // step_a, 4), lax.rem(me // step_b, 4)
@@ -139,11 +146,6 @@
             arrived(place(da, db), None)
             pass_on(place(da, db), 1 if db == 1 else 0, place(0, -db))
 
-    def gather_first():
-        for da in (1, -1):
-            pass_on(me, None, place(da, 0))
-        to_b(0)
-
     def gather_second():
         for da in (1, -1):
             arrived(place(da, 0), None)
@@ -162,9 +164,11 @@
             for side in (0, 1):
                 arrived(place(da, 2), side)
 
+    for da in (1, -1):
+        pass_on(me, None, place(da, 0))
     for d in range(1, n):
         send_tok(d).start()
-    gather_first()
+    to_b(0)
 
     keys = unit(ekeys[...].astype(F32))
     ek[...] = keys
@@ -204,7 +208,6 @@
         return 0
 
     lax.fori_loop(0, 8, recall, 0)
-    gather_second()
 
     for h in range(4):
         b = rate1[:, h : h + 1]
@@ -215,7 +218,7 @@
         u = rhs + mm(nilpotent(a).astype(BF16), rhs.astype(BF16))
         r1[h] = u * jnp.exp(tot1[:, h : h + 1] - c_col)
 
-    gather_third()
+    gather_second()
     own = lax.broadcasted_iota(jnp.int32, (16, 128), 0) // 4
 
     def fold(t, _):
@@ -231,8 +234,17 @@
         return 0
 
     lax.fori_loop(0, 8, fold, 0)
-    relay_b(1)
-    relay_b(-1)
+    for g in range(n // 4):
+        group = lax.rem(me // 4 + g, n // 4)
+        for i in range(4):
+            src = 4 * group + i
+
+            @pl.when(src != me)
+            def _():
+                to_peer(tok.at[pl.ds(0, 64), :], x.at[src, half, :], tsend.at[0], trecv.at[src], src).wait_recv()
+
+        share(g).start()
+    gather_third()
 
     for c in load_w:
         c.wait()
@@ -241,13 +253,7 @@
     ssq[...] = jnp.zeros_like(ssq)
     for g in range(n // 4):
         group = lax.rem(me // 4 + g, n // 4)
-        for i in range(4):
-            src = 4 * group + i
-
-            @pl.when(src != me)
-            def _():
-                to_peer(tok.at[pl.ds(0, 128), :], x.at[src], tsend.at[0], trecv.at[src], src).wait_recv()
-
+        share(g).wait_recv()
         pieces = []
         square = jnp.zeros((128, 128), F32)
         for i in range(4):
@@ -261,7 +267,8 @@
         scal[1] += mm_nt(scaled, decay_t[:, cols])
         for i in range(4):
             proj[i] += mm(scaled, w[i, cols, :])
-    relay_b(2)
+    relay_b(1)
+    relay_b(-1)
     inverse = lax.rsqrt(jnp.sum(ssq[...], axis=1, keepdims=True) / width + 1e-06)
     beta_raw = scal[0] * inverse
     decay_raw = scal[1] * inverse
@@ -284,6 +291,7 @@
         return 0
 
     lax.fori_loop(0, 8, recall_new, 0)
+    relay_b(2)
 
     upper = core > 0
     pos = lax.broadcasted_iota(jnp.int32, (128, 1), 0) % 4
@@ -327,7 +335,6 @@
             both = part[i] + precv[i].astype(F32)
             squares = squares + both * both
     factor = lax.rsqrt(jnp.sum(squares, axis=0, keepdims=True) / width + 1e-06)
-    half = pl.ds(pl.multiple_of(core * 64, 64), 64)
     for i in range(n):
         both = part[i, half, :] + precv[i, half, :].astype(F32)
         msend[i] = (both * factor).astype(BF16)
@@ -347,6 +354,8 @@
         send_out(d).wait_send()
     for c in range(4):
         swap(c).wait_send()
+    for g in range(n // 4):
+        share(g).wait_send()
     for copy in sent:
         copy.wait_send()
 
@@ -405,7 +414,7 @@
             VM((n, 128, 128), BF16),
             VM((n, 128, 128), BF16),
             VM((n, 64, 128), BF16),
-            dma, dma, dma((8,)), dma((4,)), dma((n,)), dma((n,)), dma((20,)), dma((n, 2)), dma((4,)), dma((4,)), dma((n,)), dma((n,)),
+            dma, dma, dma((8,)), dma((4,)), dma((n,)), dma((n,)), dma((20,)), dma((n, 2)), dma((4,)), dma((4,)), dma((n,)), dma((n,)), dma((4,)), dma((4,)),
         ],
         compiler_params=pltpu.CompilerParams(collective_id=0, has_side_effects=True, vmem_limit_bytes=48 << 20),
         name="delta_step",

time: 47.9 us -> 41.2 us (0.86)
  Pallas kernels: 47.1 us -> 40.4 us
    pallas_call x1, Pallas kernels: 43 us -> 36.3 us  [local(): pl.pallas_call(functools.partial(main_kernel, n), out_shape=(VM(saved_sta...]
where the time goes in v3:
time: 41.2 us; the launch traced here: 41.1 us
  Pallas kernels  40.4 us (98%)
  between operations  0.66 us (2%)
    pallas_call x1, Pallas kernels, local(): pl.pallas_call(functools.partial(main_kernel, n), out_shape=(VM(saved_sta...  36.3 us
    pallas_call x1, Pallas kernels, local(): pl.pallas_call(functools.partial(last_kernel, n), out_shape=(jax.ShapeDty...  4.07 us

profile of v3, /device:TPU:1, one launch (start us, length us, event | category | flops | bytes accessed | tf_op | source)
XLA Modules:
  0.0 41.1 jit_solution(15471774707843375915)
XLA Ops:
  0.6 0.0 copy-start
  0.6 36.3 %delta_step.1 = (f32[32,4,128,128]{3,2,1,0:T(8,128)S(1)}, bf16[16,64,128]{2,1,0:T(8,128)(2,1)S(1)}) custom-call(bf16[2048,128]{1,0:T(8,128)(2,1)} %tokens.1, f32[16,128]{1,0:T(8,128)} %bitcast.17, bf16[2048,512]{1,0:T(8,128)(2,1)} %wq.1, bf16[2048,512]{1,0:T(8,128)(2,1)} %wk.1, bf16[2048,512]{1,0:T(8,128)(2,1)} %wv.1, bf16[2048,512]{1,0:T(8,128)(2,1)} %wg.1, ...), custom_call_target="tpu_custom_call" | custom-call | tf_op jit(solution)/shard_map/delta_step/pallas_call | solution.py:386
  37.0 0.0 copy-done
  37.0 4.1 %write_out.1 = (f32[32,4,128,128]{3,2,1,0:T(8,128)}, bf16[64,2048]{1,0:T(8,128)(2,1)}) custom-call(f32[32,4,128,128]{3,2,1,0:T(8,128)S(1)} %get-tuple-element.6.state, bf16[16,64,128]{2,1,0:T(8,128)(2,1)S(1)} %get-tuple-element.7.mixed_in, f32[1,64]{1,0:T(1,128)S(1)} %bitcast.12), custom_call_target="tpu_custom_call" | custom-call | tf_op jit(solution)/shard_map/write_out/pallas_call | solution.py:427
Async XLA Ops:
  0.6 36.3 %copy-start = (f32[64]{0:T(128)S(1)}, f32[64]{0:T(128)}, u32[]{:S(2)}) copy-start(f32[64]{0:T(128)} %param.29) | copy-start | bytes 772

commit v4 on v1

v4 whole, which is shorter than its diff:
```python
import functools

import jax
import jax.numpy as jnp
from jax import lax
from jax.experimental import pallas as pl
from jax.experimental.pallas import tpu as pltpu
from jax.sharding import PartitionSpec as P

MESH = pl.DeviceIdType.MESH
F32 = jnp.float32
BF16 = jnp.bfloat16
HIGH = lax.Precision.HIGHEST
VM = pltpu.VMEM
NT = (((1,), (1,)), ((), ()))
TN = (((0,), (0,)), ((), ()))


def mm(a, b):
    return jnp.dot(a, b, preferred_element_type=F32)


def mm_nt(a, b):
    return lax.dot_general(a, b, NT, preferred_element_type=F32)


def silu(v):
    return v / (1.0 + jnp.exp(-v))


def unit(v):
    return v * lax.rsqrt(jnp.sum(v * v, axis=-1, keepdims=True) + 1e-06)


def quad_rows(wide, rows):
    own = lax.broadcasted_iota(jnp.int32, (rows, 128), 0) % 16 // 4
    out = wide[:, 0:128]
    for q in range(1, 4):
        out = jnp.where(own == q, wide[:, 128 * q : 128 * q + 128], out)
    return out


def masks():
    r = lax.broadcasted_iota(jnp.int32, (128, 128), 0)
    c = lax.broadcasted_iota(jnp.int32, (128, 128), 1)
    same = r // 4 == c // 4
    return r == c, same, same & (c < r), same & (c <= r)


def as_row(col, eye):
    return jnp.sum(jnp.where(eye, col, 0.0), axis=0, keepdims=True)


def ratios(c_col, c_row, keep):
    return jnp.where(keep, jnp.exp(jnp.where(keep, c_col - c_row, 0.0)), 0.0)


def nilpotent(a):
    ab = a.astype(BF16)
    square = mm(ab, ab)
    return square - a - mm(ab, square.astype(BF16))


def main_kernel(
    n,
    tokens, out_w, saved, wq, wk, wv, wg,
    ekeys_in, evals_in, erates_in, edecays_in, accepted_in, pre_gain_in, beta_in, decay_in, decay_log_in, head_gain_in,
    state, mixed_in, sums, k1b, u1, tot,
    ekeys, evals, erates, edecays, accepted, pre_gain, beta_t, decay_t, decay_log, head_gain,
    tok, x, w, ow, wt, state_b, ek, ev, r1, rq, k2b, q2b, v2, gates, proj, scal, ssq, att,
    part, psend, precv, msend,
    tok_sem, ow_sem, s_sem, w_sem, small_sem, tsend, trecv, gsend, grecv, xsend, xrecv, osend, orecv, fsend, frecv,
    asend, arecv, ssend, srecv,
):
    me = lax.axis_index("kv")
    core = lax.axis_index("tp")
    width = n * 128

    barrier = pltpu.get_barrier_semaphore()
    for d in range(1, n):
        pl.semaphore_signal(barrier, inc=1, device_id={"kv": lax.rem(me + d, n), "tp": core}, device_id_type=MESH)
    pl.semaphore_signal(barrier, inc=1, device_id={"kv": me, "tp": 1 - core}, device_id_type=MESH)

    load_tok = pltpu.make_async_copy(tokens, tok, tok_sem)
    load_ow = pltpu.make_async_copy(out_w, ow, ow_sem)
    load_ow.start()
    load_tok.start()
    small = (
        (ekeys_in, ekeys), (evals_in, evals), (erates_in, erates), (edecays_in, edecays), (accepted_in, accepted),
        (pre_gain_in, pre_gain), (beta_in, beta_t), (decay_in, decay_t), (decay_log_in, decay_log), (head_gain_in, head_gain),
    )
    load_small = [pltpu.make_async_copy(src, dst, small_sem.at[i]) for i, (src, dst) in enumerate(small)]
    for c in load_small:
        c.start()

    def load_s(t):
        some = pl.ds(4 * t, 4)
        return pltpu.make_async_copy(saved.at[some], state.at[some], s_sem.at[t])

    load_w = [pltpu.make_async_copy(src, w.at[i], w_sem.at[i]) for i, src in enumerate((wq, wk, wv, wg))]

    eye, same, strict, incl = masks()
    load_ow.wait()
    load_tok.wait()
    for c in load_small:
        c.wait()
    for t in range(8):
        load_s(t).start()
    wt[pl.ds(me, 1)] = mm_nt(jnp.where(eye, 1.0, 0.0).astype(BF16), ow[...]).astype(BF16)[None]
    half = pl.ds(pl.multiple_of(core * 64, 64), 64)
    x[pl.ds(me, 1), half, :] = tok[pl.ds(pl.multiple_of(me * 128 + core * 64, 64), 64), :][None]

    keys = unit(ekeys[...].astype(F32))
    ek[...] = keys
    ev[...] = evals[...].astype(F32)
    count = accepted[...]
    total = jnp.zeros((4, 32), F32)
    rate_p, cum_p = [], []
    for p in range(4):
        live = jnp.where(p < count, 1.0, 0.0)
        total = total + edecays[p] * live
        rate_p.append(erates[p] * live)
        cum_p.append(total)
    row = lax.broadcasted_iota(jnp.int32, (128, 32), 0)
    seq = lax.broadcasted_iota(jnp.int32, (128, 32), 1)

    def expand(pieces):
        out = jnp.zeros((128, 4), F32)
        for p in range(4):
            pick = jnp.where(row == 4 * seq + p, 1.0, 0.0)
            out = out + lax.dot_general(pick, pieces[p], NT, precision=HIGH, preferred_element_type=F32)
        return out

    rate1 = expand(rate_p)
    cum1 = expand(cum_p)
    tot1 = expand([total] * 4)
    pl.semaphore_wait(barrier, n)

    def to_peer(src, dst, ssem, rsem, peer):
        return pltpu.make_async_remote_copy(
            src_ref=src, dst_ref=dst, send_sem=ssem, recv_sem=rsem,
            device_id={"kv": peer, "tp": core}, device_id_type=MESH,
        )

    def send_tok(d):
        peer = lax.rem(me + d, n)
        rows = pl.ds(pl.multiple_of(peer * 128 + core * 64, 64), 64)
        return to_peer(tok.at[rows, :], x.at[me, half, :], tsend, trecv.at[me // 4], peer)

    def share(g):
        some = x.at[pl.ds(4 * lax.rem(me // 4 + g, n // 4), 4), half, :]
        return pltpu.make_async_remote_copy(
            src_ref=some, dst_ref=some, send_sem=fsend, recv_sem=frecv.at[g],
            device_id={"kv": me, "tp": 1 - core}, device_id_type=MESH,
        )

    at_z, at_y = me // 4, lax.rem(me, 4)
    pair = me + 1 - 2 * lax.rem(at_y, 2)

    def place(dz, side):
        return lax.rem(at_z + dz, n // 4) * 4 + at_y + side * (3 - 2 * at_y)

    def pass_on(block, peer):
        return to_peer(wt.at[block], wt.at[block], gsend, grecv.at[block], peer)

    def arrived(block):
        pass_on(block, me).wait_recv()

    far = [dz for dz in (2, 1, 3) if dz < n // 4]

    def gather_first():
        pass_on(me, place(0, 1)).start()
        for dz in far:
            pass_on(me, place(dz, 0)).start()

    def gather_second():
        arrived(place(0, 1))
        for dz in far:
            along, across = place(dz, 0), place(0, 1)
            arrived(along)
            pass_on(across + core * (along - across), along + core * (across - along)).start()

    for d in range(1, n):
        send_tok(d).start()
    gather_first()
    for c in load_w:
        c.start()

    for h in range(4):
        k1b[h] = ek[pl.ds(h, 128, stride=4), :].astype(BF16)
        tot[h] = jnp.broadcast_to(jnp.exp(tot1[:, h : h + 1]), (128, 128))

    def recall(t, _):
        load_s(t).wait()
        rows = pl.ds(pl.multiple_of(16 * t, 16), 16)
        for h in range(4):
            wide = jnp.concatenate([state[4 * t + q, h].astype(BF16) for q in range(4)], axis=1)
            state_b[h, t] = wide
            r1[h, rows, :] = quad_rows(mm(k1b[h, rows, :], wide), 16)
        return 0

    lax.fori_loop(0, 8, recall, 0)

    for h in range(4):
        b = rate1[:, h : h + 1]
        c_col = cum1[:, h : h + 1]
        kb = k1b[h]
        a = b * ratios(c_col, as_row(c_col, eye), strict) * mm_nt(kb, kb)
        rhs = b * (ev[pl.ds(h, 128, stride=4), :] - jnp.exp(c_col) * r1[h])
        u = rhs + mm(nilpotent(a).astype(BF16), rhs.astype(BF16))
        u1[h] = u * jnp.exp(tot1[:, h : h + 1] - c_col)

    def collect(g):
        group = lax.rem(me // 4 + g, n // 4)
        count = 4 if g else 3
        rows = tok.at[pl.ds(0, 64 * count), :]
        to_peer(rows, rows, tsend, trecv.at[group], me).wait_recv()
        share(g).start()

    def project(g):
        group = lax.rem(me // 4 + g, n // 4)
        share(g).wait_recv()
        pieces = []
        square = jnp.zeros((128, 128), F32)
        for i in range(4):
            wide = x[pl.ds(4 * group + i, 1)][0].astype(F32)
            square = square + wide * wide
            pieces.append((wide * pre_gain[pl.ds(4 * group + i, 1), :]).astype(BF16))
        scaled = jnp.concatenate(pieces, axis=1)
        cols = pl.ds(pl.multiple_of(group * 512, 512), 512)
        beta = mm_nt(scaled, beta_t[:, cols])
        decay = mm_nt(scaled, decay_t[:, cols])
        ssq[...] = square if g == 0 else ssq[...] + square
        scal[0] = beta if g == 0 else scal[0] + beta
        scal[1] = decay if g == 0 else scal[1] + decay
        for i in range(4):
            out = mm(scaled, w[i, cols, :])
            proj[i] = out if g == 0 else proj[i] + out

    groups = n // 4
    for c in load_w:
        c.wait()
    for g in range(groups):
        collect(g)
        if g > 1:
            project(g - 2)
    for g in range(max(groups - 2, 0), groups):
        project(g)
    inverse = lax.rsqrt(jnp.sum(ssq[...], axis=1, keepdims=True) / width + 1e-06)
    beta_raw = scal[0] * inverse
    decay_raw = scal[1] * inverse
    rates8 = 1.0 / (1.0 + jnp.exp(-beta_raw))
    soft8 = jnp.maximum(decay_raw, 0.0) + jnp.log1p(jnp.exp(-jnp.abs(decay_raw)))
    for h in range(4):
        lanes = slice(128 * h, 128 * h + 128)
        q2b[h] = (unit(silu(proj[0, :, lanes] * inverse)) * 128 ** (-0.5)).astype(BF16)
        k2b[h] = unit(silu(proj[1, :, lanes] * inverse)).astype(BF16)
        v2[h] = silu(proj[2, :, lanes] * inverse)
        gates[h] = silu(proj[3, :, lanes] * inverse) * head_gain[...]

    def recall_new(t, _):
        rows = pl.ds(pl.multiple_of(16 * t, 16), 16)
        for h in range(4):
            both = jnp.concatenate([k2b[h, rows, :], q2b[h, rows, :]], axis=0)
            out = quad_rows(mm(both, state_b[h, t]), 32)
            r1[h, rows, :] = out[:16]
            rq[h, rows, :] = out[16:]
        return 0

    lax.fori_loop(0, 8, recall_new, 0)
    gather_second()

    def to_pair(h):
        two = pl.ds(2 * h, 2)
        return to_peer(att.at[0, two], att.at[1, two], asend, arecv, pair)

    upper = core > 0
    pos = lax.broadcasted_iota(jnp.int32, (128, 1), 0) % 4
    for h in range(4):
        b = jnp.where(upper, rates8[:, h + 4 : h + 5], rates8[:, h : h + 1])
        g = jnp.where(upper, soft8[:, h + 4 : h + 5], soft8[:, h : h + 1])
        g = -jnp.exp(decay_log[:, h : h + 1]) * g
        c_col = jnp.sum(jnp.where(incl, as_row(g, eye), 0.0), axis=1, keepdims=True)
        ratio = ratios(c_col, as_row(c_col, eye), incl)
        kb, kept = k2b[h], tot[h]
        cross = mm_nt(jnp.concatenate([kb, q2b[h]], axis=0), jnp.concatenate([kb, k1b[h]], axis=0))
        a = jnp.where(strict, b * ratio * cross[:128, :128], 0.0)
        seen = ratio * cross[128:, :128]
        past = jnp.concatenate([jnp.where(same, cross[:128, 128:], 0.0), jnp.where(same, cross[128:, 128:], 0.0)], axis=0)
        past = mm(past.astype(BF16), u1[h].astype(BF16))
        recalled = kept * r1[h] + past[:128]
        queried = kept * rq[h] + past[128:]
        seen = seen + mm(seen.astype(BF16), nilpotent(a).astype(BF16))
        grown = jnp.exp(c_col)
        rhs = b * (v2[h] - grown * recalled)
        reads = grown * queried + mm(seen.astype(BF16), rhs.astype(BF16))
        normed = reads * lax.rsqrt(jnp.mean(reads * reads, axis=-1, keepdims=True) + 1e-06)
        att[0, h] = (normed * gates[h]).astype(BF16)
        if h % 2:
            to_pair(h // 2).start()

    def swap(c):
        part_sum = slice(None) if c is None else c
        return pltpu.make_async_remote_copy(
            src_ref=psend.at[part_sum], dst_ref=precv.at[part_sum], send_sem=xsend, recv_sem=xrecv,
            device_id={"kv": me, "tp": 1 - core}, device_id_type=MESH,
        )

    to_peer(att.at[0], att.at[1], asend, arecv, pair).wait()
    attended = jnp.concatenate([jnp.concatenate([att[i, h] for h in range(4)], axis=1) for i in range(2)], axis=0)
    blocks = [(dz, side) for side in range(2) for dz in [0] + far]
    many = n // 4
    for side in range(2):
        for dz in far if side else ():
            arrived(place(dz, side))
        some = jnp.concatenate([wt[pl.ds(place(dz, side), 1)][0] for dz in [0] + far], axis=0)
        out = mm_nt(some, attended).reshape(many, 128, 256)
        rows = pl.ds(side * many, many)
        part[rows] = out
        psend[rows] = out.astype(BF16)
        swap(rows).start()
    swap(None).wait_recv()
    squares = jnp.zeros((128, 256), F32)
    for i in range(n // 2):
        both = part[i] + precv[i].astype(F32)
        squares = squares + both * both
        part[i] = both
    squares = jnp.sum(squares, axis=0, keepdims=True)
    first = lax.broadcasted_iota(jnp.int32, (8, 128), 0) == 0
    sums[pl.ds(me, 1)] = jnp.where(first, squares[:, :128], squares[:, 128:])[None]

    def send_sums(d):
        peer = lax.rem(me + d, n)
        return to_peer(sums.at[me], sums.at[me], ssend, srecv, peer)

    for d in range(1, n):
        send_sums(d).start()
    for i in range(n // 2):
        both = part[i, half, :].astype(BF16)
        msend[0, i] = both[:, :128]
        msend[1, i] = both[:, 128:]
    mixed_in[pl.ds(me, 1)] = msend[0, 0][None]
    mixed_in[pl.ds(pair, 1)] = msend[1, 0][None]
    for i, (dz, side) in enumerate(blocks):
        if i:
            peer = place(dz, side)
            to_peer(msend.at[0, i], mixed_in.at[me], osend, orecv, peer).start()
            to_peer(msend.at[1, i], mixed_in.at[pair], osend, orecv, peer).start()
    others = pl.ds(0, n - 2)
    to_peer(mixed_in.at[others], mixed_in.at[others], osend, orecv, me).wait()
    others = pl.ds(0, n - 1)
    to_peer(sums.at[others], sums.at[others], ssend, srecv, me).wait()
    rows = tok.at[pl.ds(0, 64 * (n - 1)), :]
    to_peer(rows, rows, tsend, tsend, me).wait_send()
    mine = x.at[:, half, :]
    to_peer(mine, mine, fsend, fsend, me).wait_send()
    others = pl.ds(0, 1 + 2 * len(far))
    to_peer(wt.at[others], wt.at[others], gsend, gsend, me).wait_send()
    swap(None).wait_send()


def last_kernel(n, state, k1b, u1, tot, mixed_in, sums, post_gain, committed, mixed, new, rows_out, sem, mixed_sem):
    i = lax.broadcasted_iota(jnp.int32, (64, 64), 0)
    j = lax.broadcasted_iota(jnp.int32, (64, 64), 1)
    gain = jnp.sum(jnp.where(i == j, post_gain[...], 0.0), axis=1, keepdims=True)
    for k in range(n):
        total = sums[k, 0:1, :] + sums[k + 1 - 2 * (k % 2), 1:2, :]
        factor = lax.rsqrt(total / (n * 128) + 1e-06)
        rows_out[:, 128 * k : 128 * k + 128] = (mixed_in[k].astype(F32) * factor * gain).astype(BF16)
    write_mixed = pltpu.make_async_copy(rows_out, mixed, mixed_sem)
    write_mixed.start()
    own = lax.broadcasted_iota(jnp.int32, (16, 128), 0) // 4

    def write(t):
        some = pl.ds(4 * t, 4)
        return pltpu.make_async_copy(new.at[some], committed.at[some], sem.at[t])

    def fold(t, _):
        rows = pl.ds(pl.multiple_of(16 * t, 16), 16)
        for h in range(4):
            u = u1[h, rows, :]
            wide = jnp.concatenate([jnp.where(own == q, u, 0.0) for q in range(4)], axis=1).astype(BF16)
            step = lax.dot_general(k1b[h, rows, :], wide, TN, preferred_element_type=F32)
            for q in range(4):
                kept = state[4 * t + q, h] * tot[h, pl.ds(16 * t + 4 * q, 1), :]
                new[4 * t + q, h] = kept + step[:, 128 * q : 128 * q + 128]
        write(t).start()
        return 0

    lax.fori_loop(0, 8, fold, 0)
    for t in range(8):
        write(t).wait()
    write_mixed.wait()


def local(
    n,
    tokens, pre_gain, query_weight, key_weight, value_weight, gate_weight, beta_weight, decay_weight, decay_log,
    head_gain, out_weight, post_gain, saved_state, earlier_keys, earlier_values, earlier_rates, earlier_decays, accepted,
):
    any_spec = pl.BlockSpec(memory_space=pl.ANY)
    vmem = pl.BlockSpec(memory_space=VM)
    dma = pltpu.SemaphoreType.DMA
    heads = (4, 128, 128)
    state, mixed_in, sums, k1b, u1, tot = pl.pallas_call(
        functools.partial(main_kernel, n),
        out_shape=(VM(saved_state.shape, F32), VM((n, 64, 128), BF16), VM((n, 8, 128), F32), VM(heads, BF16), VM(heads, F32), VM(heads, F32)),
        in_specs=[any_spec] * 17,
        out_specs=(vmem,) * 6,
        scratch_shapes=[
            VM((512, 128), BF16),
            VM((512, 128), BF16),
            VM((4, 4, 32), F32),
            VM((4, 4, 32), F32),
            VM((1, 32), jnp.int32),
            VM((n, 128), F32),
            VM((8, n * 128), BF16),
            VM((8, n * 128), BF16),
            VM((1, 4), F32),
            VM((1, 128), F32),
            VM((n * 128, 128), BF16),
            VM((n, 128, 128), BF16),
            VM((4, n * 128, 512), BF16),
            VM((512, 128), BF16),
            VM((n, 128, 512), BF16),
            VM((4, 8, 128, 512), BF16),
            VM((512, 128), F32),
            VM((512, 128), F32),
            VM(heads, F32),
            VM(heads, F32),
            VM(heads, BF16),
            VM(heads, BF16),
            VM(heads, F32),
            VM(heads, F32),
            VM((4, 128, 512), F32),
            VM((2, 128, 8), F32),
            VM((128, 128), F32),
            VM((2, 4, 128, 128), BF16),
            VM((n // 2, 128, 256), F32),
            VM((n // 2, 128, 256), BF16),
            VM((n // 2, 128, 256), BF16),
            VM((2, n // 2, 64, 128), BF16),
            dma, dma, dma((8,)), dma((4,)), dma((10,)),
            dma, dma((n // 4,)), dma, dma((n,)), dma, dma, dma, dma, dma, dma((n // 4,)), dma, dma, dma, dma,
        ],
        compiler_params=pltpu.CompilerParams(collective_id=0, has_side_effects=True, vmem_limit_bytes=48 << 20),
        name="delta_step",
    )(
        tokens, out_weight, saved_state, query_weight, key_weight, value_weight, gate_weight,
        earlier_keys.reshape(512, 128), earlier_values.reshape(512, 128), earlier_rates.transpose(1, 2, 0),
        earlier_decays.transpose(1, 2, 0), accepted.reshape(1, 32), pre_gain.reshape(n, 128), beta_weight.T,
        decay_weight.T, decay_log.reshape(1, 4), head_gain.reshape(1, 128),
    )
    committed, mixed = pl.pallas_call(
        functools.partial(last_kernel, n),
        out_shape=(jax.ShapeDtypeStruct(saved_state.shape, F32), jax.ShapeDtypeStruct((64, n * 128), BF16)),
        in_specs=[vmem] * 7,
        out_specs=(any_spec, any_spec),
        scratch_shapes=[VM(saved_state.shape, F32), VM((64, n * 128), BF16), dma((8,)), dma],
        compiler_params=pltpu.CompilerParams(vmem_limit_bytes=32 << 20),
        name="write_out",
    )(state, k1b, u1, tot, mixed_in, sums, post_gain.reshape(1, 64))
    return mixed.T, committed


def solution(mesh):
    placed = (
        P("dp", "kv"), P(), P(None, "tp"), P(None, "tp"), P(None, "tp"), P(None, "tp"), P(), P(), P("tp"), P(),
        P("tp", "kv"), P(("kv", "tp")), P(("dp", "kv"), "tp", None, None), P(("dp", "kv"), None, "tp", None),
        P(("dp", "kv"), None, "tp", None), P(("dp", "kv"), None, "tp"), P(("dp", "kv"), None, "tp"), P(("dp", "kv")),
    )
    return jax.shard_map(
        functools.partial(local, mesh.shape["kv"]),
        mesh=mesh,
        in_specs=placed,
        out_specs=(P("dp", ("kv", "tp")), P(("dp", "kv"), "tp", None, None)),
        check_vma=False,
    )
```

time: 59.8 us -> 38.3 us (0.64)
  Pallas kernels: 59 us -> 37.5 us
    pallas_call x1, Pallas kernels: 55 us -> 33.7 us  [local(): pl.pallas_call(functools.partial(main_kernel, n), out_shape=(VM(saved_sta...]
where the time goes in v4:
time: 38.3 us; the launch traced here: 38.2 us
  Pallas kernels  37.5 us (98%)
  between operations  0.66 us (2%)
    pallas_call x1, Pallas kernels, local(): pl.pallas_call(functools.partial(main_kernel, n), out_shape=(VM(saved_sta...  33.7 us
    pallas_call x1, Pallas kernels, local(): pl.pallas_call(functools.partial(last_kernel, n), out_shape=(jax.ShapeDty...  3.82 us

profile of v4, /device:TPU:1, one launch (start us, length us, event | category | flops | bytes accessed | tf_op | source)
XLA Modules:
  0.0 38.2 jit_solution(8750252911070729816)
XLA Ops:
  0.6 0.0 copy-start
  0.6 33.7 %delta_step.1 = (f32[32,4,128,128]{3,2,1,0:T(8,128)S(1)}, bf16[16,64,128]{2,1,0:T(8,128)(2,1)S(1)}, f32[16,8,128]{2,1,0:T(8,128)S(1)}, bf16[4,128,128]{2,1,0:T(8...) custom-call(bf16[2048,128]{1,0:T(8,128)(2,1)} %tokens.1, bf16[512,128]{1,0:T(8,128)(2,1)} %out_w.1, ...), custom_call_target="tpu_custom_call" | custom-call | tf_op jit(solution)/shard_map/delta_step/pallas_call | solution.py:405
  34.3 0.0 copy-done
  34.4 3.8 %write_out.1 = (f32[32,4,128,128]{3,2,1,0:T(8,128)}, bf16[64,2048]{1,0:T(8,128)(2,1)}) custom-call(f32[32,4,128,128]{3,2,1,0:T(8,128)S(1)} %get-tuple-element.10.state, bf16[4,128,128]{2,1,0:T(8,128)(2,1)S(1)} %get-tuple-element.11.k1b, f32[4,128,128]{2,1,0:T(8,128)S(1)} %get-tuple-element.12.u1, f32[4,128,128]{2,1,0:T(8,128)S(1)} %get-tuple-element.13.tot, ...), custom_call_target="tpu_custom_call" | custom-call | tf_op jit(solution)/shard_map/write_out/pallas_call | solution.py:454
Async XLA Ops:
  0.6 33.7 %copy-start = (f32[64]{0:T(128)S(1)}, f32[64]{0:T(128)}, u32[]{:S(2)}) copy-start(f32[64]{0:T(128)} %param.29) | copy-start | bytes 772

commit v5 on v4

--- a/solution.py
+++ b/solution.py
@@ -44,7 +44,7 @@
     r = lax.broadcasted_iota(jnp.int32, (128, 128), 0)
     c = lax.broadcasted_iota(jnp.int32, (128, 128), 1)
     same = r // 4 == c // 4
-    return r == c, same, same & (c < r), same & (c <= r)
+    return r == c, same & (c < r), same & (c <= r)
 
 
 def as_row(col, eye):
@@ -65,9 +65,9 @@
     n,
     tokens, out_w, saved, wq, wk, wv, wg,
     ekeys_in, evals_in, erates_in, edecays_in, accepted_in, pre_gain_in, beta_in, decay_in, decay_log_in, head_gain_in,
-    state, mixed_in, sums, k1b, u1, tot,
+    state, mixed_in, sums,
     ekeys, evals, erates, edecays, accepted, pre_gain, beta_t, decay_t, decay_log, head_gain,
-    tok, x, w, ow, wt, state_b, ek, ev, r1, rq, k2b, q2b, v2, gates, proj, scal, ssq, att,
+    tok, x, w, ow, wt, state_b, ek, ev, k1b, u1, tot, r1, rq, k2b, q2b, v2, gates, proj, scal, ssq, att,
     part, psend, precv, msend,
     tok_sem, ow_sem, s_sem, w_sem, small_sem, tsend, trecv, gsend, grecv, xsend, xrecv, osend, orecv, fsend, frecv,
     asend, arecv, ssend, srecv,
@@ -99,7 +99,7 @@
 
     load_w = [pltpu.make_async_copy(src, w.at[i], w_sem.at[i]) for i, src in enumerate((wq, wk, wv, wg))]
 
-    eye, same, strict, incl = masks()
+    eye, strict, incl = masks()
     load_ow.wait()
     load_tok.wait()
     for c in load_small:
@@ -168,10 +168,15 @@
 
     far = [dz for dz in (2, 1, 3) if dz < n // 4]
 
-    def gather_first():
-        pass_on(me, place(0, 1)).start()
-        for dz in far:
-            pass_on(me, place(dz, 0)).start()
+    def gather_first(along):
+        @pl.when(core == along)
+        def _():
+            for dz in far:
+                pass_on(me, place(dz, 0)).start()
+
+        @pl.when(core != along)
+        def _():
+            pass_on(me, place(0, 1)).start()
 
     def gather_second():
         arrived(place(0, 1))
@@ -182,7 +187,7 @@
 
     for d in range(1, n):
         send_tok(d).start()
-    gather_first()
+    gather_first(1)
     for c in load_w:
         c.start()
 
@@ -195,11 +200,11 @@
         rows = pl.ds(pl.multiple_of(16 * t, 16), 16)
         for h in range(4):
             wide = jnp.concatenate([state[4 * t + q, h].astype(BF16) for q in range(4)], axis=1)
-            state_b[h, t] = wide
             r1[h, rows, :] = quad_rows(mm(k1b[h, rows, :], wide), 16)
         return 0
 
-    lax.fori_loop(0, 8, recall, 0)
+    lax.fori_loop(0, 8, recall, 0, unroll=2)
+    gather_first(0)
 
     for h in range(4):
         b = rate1[:, h : h + 1]
@@ -209,6 +214,23 @@
         rhs = b * (ev[pl.ds(h, 128, stride=4), :] - jnp.exp(c_col) * r1[h])
         u = rhs + mm(nilpotent(a).astype(BF16), rhs.astype(BF16))
         u1[h] = u * jnp.exp(tot1[:, h : h + 1] - c_col)
+
+    own = lax.broadcasted_iota(jnp.int32, (16, 128), 0) // 4
+
+    def fold(t, _):
+        rows = pl.ds(pl.multiple_of(16 * t, 16), 16)
+        for h in range(4):
+            u = u1[h, rows, :]
+            wide = jnp.concatenate([jnp.where(own == q, u, 0.0) for q in range(4)], axis=1).astype(BF16)
+            step = lax.dot_general(k1b[h, rows, :], wide, TN, preferred_element_type=F32)
+            for q in range(4):
+                kept = state[4 * t + q, h] * tot[h, pl.ds(16 * t + 4 * q, 1), :]
+                new = kept + step[:, 128 * q : 128 * q + 128]
+                state[4 * t + q, h] = new
+                state_b[h, t, :, 128 * q : 128 * q + 128] = new.astype(BF16)
+        return 0
+
+    lax.fori_loop(0, 8, fold, 0, unroll=2)
 
     def collect(g):
         group = lax.rem(me // 4 + g, n // 4)
@@ -238,10 +260,11 @@
             proj[i] = out if g == 0 else proj[i] + out
 
     groups = n // 4
-    for c in load_w:
-        c.wait()
     for g in range(groups):
         collect(g)
+        if g == min(1, groups - 1):
+            for c in load_w:
+                c.wait()
         if g > 1:
             project(g - 2)
     for g in range(max(groups - 2, 0), groups):
@@ -267,85 +290,81 @@
             rq[h, rows, :] = out[16:]
         return 0
 
-    lax.fori_loop(0, 8, recall_new, 0)
     gather_second()
+    lax.fori_loop(0, 8, recall_new, 0, unroll=2)
 
     def to_pair(h):
         two = pl.ds(2 * h, 2)
         return to_peer(att.at[0, two], att.at[1, two], asend, arecv, pair)
 
     upper = core > 0
-    pos = lax.broadcasted_iota(jnp.int32, (128, 1), 0) % 4
     for h in range(4):
         b = jnp.where(upper, rates8[:, h + 4 : h + 5], rates8[:, h : h + 1])
         g = jnp.where(upper, soft8[:, h + 4 : h + 5], soft8[:, h : h + 1])
         g = -jnp.exp(decay_log[:, h : h + 1]) * g
         c_col = jnp.sum(jnp.where(incl, as_row(g, eye), 0.0), axis=1, keepdims=True)
         ratio = ratios(c_col, as_row(c_col, eye), incl)
-        kb, kept = k2b[h], tot[h]
-        cross = mm_nt(jnp.concatenate([kb, q2b[h]], axis=0), jnp.concatenate([kb, k1b[h]], axis=0))
-        a = jnp.where(strict, b * ratio * cross[:128, :128], 0.0)
-        seen = ratio * cross[128:, :128]
-        past = jnp.concatenate([jnp.where(same, cross[:128, 128:], 0.0), jnp.where(same, cross[128:, 128:], 0.0)], axis=0)
-        past = mm(past.astype(BF16), u1[h].astype(BF16))
-        recalled = kept * r1[h] + past[:128]
-        queried = kept * rq[h] + past[128:]
+        kb = k2b[h]
+        cross = mm_nt(jnp.concatenate([kb, q2b[h]], axis=0), kb)
+        a = jnp.where(strict, b * ratio * cross[:128], 0.0)
+        seen = ratio * cross[128:]
         seen = seen + mm(seen.astype(BF16), nilpotent(a).astype(BF16))
         grown = jnp.exp(c_col)
-        rhs = b * (v2[h] - grown * recalled)
-        reads = grown * queried + mm(seen.astype(BF16), rhs.astype(BF16))
+        rhs = b * (v2[h] - grown * r1[h])
+        reads = grown * rq[h] + mm(seen.astype(BF16), rhs.astype(BF16))
         normed = reads * lax.rsqrt(jnp.mean(reads * reads, axis=-1, keepdims=True) + 1e-06)
         att[0, h] = (normed * gates[h]).astype(BF16)
         if h % 2:
             to_pair(h // 2).start()
 
-    def swap(c):
-        part_sum = slice(None) if c is None else c
+    def swap(slot, blocks):
         return pltpu.make_async_remote_copy(
-            src_ref=psend.at[part_sum], dst_ref=precv.at[part_sum], send_sem=xsend, recv_sem=xrecv,
+            src_ref=psend.at[slot, blocks], dst_ref=precv.at[slot, blocks], send_sem=xsend, recv_sem=xrecv.at[slot],
             device_id={"kv": me, "tp": 1 - core}, device_id_type=MESH,
         )
 
+    many = n // 4
+
+    def multiply(slot, side):
+        attended = jnp.concatenate([att[slot, h] for h in range(4)], axis=1)
+        some = jnp.concatenate([wt[pl.ds(place(dz, side), 1)][0] for dz in [0] + far], axis=0)
+        out = mm_nt(some, attended).reshape(many, 128, 128)
+        blocks = pl.ds(side * many, many)
+        part[slot, blocks] = out
+        psend[slot, blocks] = out.astype(BF16)
+        swap(slot, blocks).start()
+
+    multiply(0, 0)
+    for dz in far:
+        arrived(place(dz, 1))
+    multiply(0, 1)
     to_peer(att.at[0], att.at[1], asend, arecv, pair).wait()
-    attended = jnp.concatenate([jnp.concatenate([att[i, h] for h in range(4)], axis=1) for i in range(2)], axis=0)
-    blocks = [(dz, side) for side in range(2) for dz in [0] + far]
-    many = n // 4
-    for side in range(2):
-        for dz in far if side else ():
-            arrived(place(dz, side))
-        some = jnp.concatenate([wt[pl.ds(place(dz, side), 1)][0] for dz in [0] + far], axis=0)
-        out = mm_nt(some, attended).reshape(many, 128, 256)
-        rows = pl.ds(side * many, many)
-        part[rows] = out
-        psend[rows] = out.astype(BF16)
-        swap(rows).start()
-    swap(None).wait_recv()
-    squares = jnp.zeros((128, 256), F32)
-    for i in range(n // 2):
-        both = part[i] + precv[i].astype(F32)
-        squares = squares + both * both
-        part[i] = both
-    squares = jnp.sum(squares, axis=0, keepdims=True)
-    first = lax.broadcasted_iota(jnp.int32, (8, 128), 0) == 0
-    sums[pl.ds(me, 1)] = jnp.where(first, squares[:, :128], squares[:, 128:])[None]
+    multiply(1, 0)
+    multiply(1, 1)
 
     def send_sums(d):
-        peer = lax.rem(me + d, n)
-        return to_peer(sums.at[me], sums.at[me], ssend, srecv, peer)
-
-    for d in range(1, n):
-        send_sums(d).start()
-    for i in range(n // 2):
-        both = part[i, half, :].astype(BF16)
-        msend[0, i] = both[:, :128]
-        msend[1, i] = both[:, 128:]
-    mixed_in[pl.ds(me, 1)] = msend[0, 0][None]
-    mixed_in[pl.ds(pair, 1)] = msend[1, 0][None]
-    for i, (dz, side) in enumerate(blocks):
-        if i:
-            peer = place(dz, side)
-            to_peer(msend.at[0, i], mixed_in.at[me], osend, orecv, peer).start()
-            to_peer(msend.at[1, i], mixed_in.at[pair], osend, orecv, peer).start()
+        return to_peer(sums.at[me], sums.at[me], ssend, srecv, lax.rem(me + d, n))
+
+    totals = []
+    for slot, target in enumerate((me, pair)):
+        swap(slot, pl.ds(0, n // 2)).wait_recv()
+        squares = jnp.zeros((128, 128), F32)
+        for i in range(n // 2):
+            both = part[slot, i] + precv[slot, i].astype(F32)
+            squares = squares + both * both
+        totals.append(jnp.sum(squares, axis=0, keepdims=True))
+        if slot:
+            first = lax.broadcasted_iota(jnp.int32, (2, 128), 0) == 0
+            sums[pl.ds(me, 1)] = jnp.where(first, totals[0], totals[1])[None]
+            for d in range(1, n):
+                send_sums(d).start()
+        for i in range(n // 2):
+            both = part[slot, i, half, :] + precv[slot, i, half, :].astype(F32)
+            msend[slot, i] = both.astype(BF16)
+        mixed_in[pl.ds(target, 1)] = msend[slot, 0][None]
+        for i, (dz, side) in enumerate([(dz, side) for side in range(2) for dz in [0] + far]):
+            if i:
+                to_peer(msend.at[slot, i], mixed_in.at[target], osend, orecv, place(dz, side)).start()
     others = pl.ds(0, n - 2)
     to_peer(mixed_in.at[others], mixed_in.at[others], osend, orecv, me).wait()
     others = pl.ds(0, n - 1)
@@ -356,10 +375,16 @@
     to_peer(mine, mine, fsend, fsend, me).wait_send()
     others = pl.ds(0, 1 + 2 * len(far))
     to_peer(wt.at[others], wt.at[others], gsend, gsend, me).wait_send()
-    swap(None).wait_send()
-
-
-def last_kernel(n, state, k1b, u1, tot, mixed_in, sums, post_gain, committed, mixed, new, rows_out, sem, mixed_sem):
+    for slot in range(2):
+        swap(slot, pl.ds(0, n // 2)).wait_send()
+
+
+def last_kernel(n, state, mixed_in, sums, post_gain, committed, mixed, rows_out, sem, mixed_sem):
+    copies = []
+    for t in range(8):
+        some = pl.ds(4 * t, 4)
+        copies.append(pltpu.make_async_copy(state.at[some], committed.at[some], sem.at[t]))
+        copies[t].start()
     i = lax.broadcasted_iota(jnp.int32, (64, 64), 0)
     j = lax.broadcasted_iota(jnp.int32, (64, 64), 1)
     gain = jnp.sum(jnp.where(i == j, post_gain[...], 0.0), axis=1, keepdims=True)
@@ -369,27 +394,8 @@
         rows_out[:, 128 * k : 128 * k + 128] = (mixed_in[k].astype(F32) * factor * gain).astype(BF16)
     write_mixed = pltpu.make_async_copy(rows_out, mixed, mixed_sem)
     write_mixed.start()
-    own = lax.broadcasted_iota(jnp.int32, (16, 128), 0) // 4
-
-    def write(t):
-        some = pl.ds(4 * t, 4)
-        return pltpu.make_async_copy(new.at[some], committed.at[some], sem.at[t])
-
-    def fold(t, _):
-        rows = pl.ds(pl.multiple_of(16 * t, 16), 16)
-        for h in range(4):
-            u = u1[h, rows, :]
-            wide = jnp.concatenate([jnp.where(own == q, u, 0.0) for q in range(4)], axis=1).astype(BF16)
-            step = lax.dot_general(k1b[h, rows, :], wide, TN, preferred_element_type=F32)
-            for q in range(4):
-                kept = state[4 * t + q, h] * tot[h, pl.ds(16 * t + 4 * q, 1), :]
-                new[4 * t + q, h] = kept + step[:, 128 * q : 128 * q + 128]
-        write(t).start()
-        return 0
-
-    lax.fori_loop(0, 8, fold, 0)
-    for t in range(8):
-        write(t).wait()
+    for c in copies:
+        c.wait()
     write_mixed.wait()
 
 
@@ -402,11 +408,11 @@
     vmem = pl.BlockSpec(memory_space=VM)
     dma = pltpu.SemaphoreType.DMA
     heads = (4, 128, 128)
-    state, mixed_in, sums, k1b, u1, tot = pl.pallas_call(
+    state, mixed_in, sums = pl.pallas_call(
         functools.partial(main_kernel, n),
-        out_shape=(VM(saved_state.shape, F32), VM((n, 64, 128), BF16), VM((n, 8, 128), F32), VM(heads, BF16), VM(heads, F32), VM(heads, F32)),
+        out_shape=(VM(saved_state.shape, F32), VM((n, 64, 128), BF16), VM((n, 2, 128), F32)),
         in_specs=[any_spec] * 17,
-        out_specs=(vmem,) * 6,
+        out_specs=(vmem,) * 3,
         scratch_shapes=[
             VM((512, 128), BF16),
             VM((512, 128), BF16),
@@ -426,6 +432,9 @@
             VM((4, 8, 128, 512), BF16),
             VM((512, 128), F32),
             VM((512, 128), F32),
+            VM(heads, BF16),
+            VM(heads, F32),
+            VM(heads, F32),
             VM(heads, F32),
             VM(heads, F32),
             VM(heads, BF16),
@@ -436,12 +445,12 @@
             VM((2, 128, 8), F32),
             VM((128, 128), F32),
             VM((2, 4, 128, 128), BF16),
-            VM((n // 2, 128, 256), F32),
-            VM((n // 2, 128, 256), BF16),
-            VM((n // 2, 128, 256), BF16),
+            VM((2, n // 2, 128, 128), F32),
+            VM((2, n // 2, 128, 128), BF16),
+            VM((2, n // 2, 128, 128), BF16),
             VM((2, n // 2, 64, 128), BF16),
             dma, dma, dma((8,)), dma((4,)), dma((10,)),
-            dma, dma((n // 4,)), dma, dma((n,)), dma, dma, dma, dma, dma, dma((n // 4,)), dma, dma, dma, dma,
+            dma, dma((n // 4,)), dma, dma((n,)), dma, dma((2,)), dma, dma, dma, dma((n // 4,)), dma, dma, dma, dma,
         ],
         compiler_params=pltpu.CompilerParams(collective_id=0, has_side_effects=True, vmem_limit_bytes=48 << 20),
         name="delta_step",
@@ -454,12 +463,12 @@
     committed, mixed = pl.pallas_call(
         functools.partial(last_kernel, n),
         out_shape=(jax.ShapeDtypeStruct(saved_state.shape, F32), jax.ShapeDtypeStruct((64, n * 128), BF16)),
-        in_specs=[vmem] * 7,
+        in_specs=[vmem] * 4,
         out_specs=(any_spec, any_spec),
-        scratch_shapes=[VM(saved_state.shape, F32), VM((64, n * 128), BF16), dma((8,)), dma],
-        compiler_params=pltpu.CompilerParams(vmem_limit_bytes=32 << 20),
+        scratch_shapes=[VM((64, n * 128), BF16), dma((8,)), dma],
+        compiler_params=pltpu.CompilerParams(vmem_limit_bytes=16 << 20),
         name="write_out",
-    )(state, k1b, u1, tot, mixed_in, sums, post_gain.reshape(1, 64))
+    )(state, mixed_in, sums, post_gain.reshape(1, 64))
     return mixed.T, committed
 
 

time: 38.3 us -> 36.4 us (0.950)
  Pallas kernels: 37.5 us -> 35.6 us
    pallas_call x1, Pallas kernels: 33.7 us -> 32.1 us  [local(): pl.pallas_call(functools.partial(main_kernel, n), out_shape=(VM(saved_sta...]
    pallas_call x1, Pallas kernels: 3.82 us -> 3.43 us  [local(): pl.pallas_call(functools.partial(last_kernel, n), out_shape=(jax.ShapeDty...]
where the time goes in v5:
time: 36.4 us; the launch traced here: 36.2 us
  Pallas kernels  35.6 us (98%)
  between operations  0.66 us (2%)
    pallas_call x1, Pallas kernels, local(): pl.pallas_call(functools.partial(main_kernel, n), out_shape=(VM(saved_sta...  32.1 us
    pallas_call x1, Pallas kernels, local(): pl.pallas_call(functools.partial(last_kernel, n), out_shape=(jax.ShapeDty...  3.43 us

profile of v5, /device:TPU:1, one launch (start us, length us, event | category | flops | bytes accessed | tf_op | source)
XLA Modules:
  0.0 36.2 jit_solution(5972508819653684525)
XLA Ops:
  0.6 0.0 copy-start
  0.6 32.1 %delta_step.1 = (f32[32,4,128,128]{3,2,1,0:T(8,128)S(1)}, bf16[16,64,128]{2,1,0:T(8,128)(2,1)S(1)}, f32[16,2,128]{2,1,0:T(2,128)S(1)}) custom-call(bf16[2048,128]{1,0:T(8,128)(2,1)} %tokens.1, bf16[512,128]{1,0:T(8,128)(2,1)} %out_w.1, f32[32,4,128,128]{3,2,1,0:T(8,128)} %saved.1, bf16[2048,512]{1,0:T(8,128)(2,1)} %wq.1, bf16[2048,512]{1,0:T(8,128)(2,1)} %wk.1, ...), custom_call_target="tpu_custom_call" | custom-call | tf_op jit(solution)/shard_map/delta_step/pallas_call | solution.py:411
  32.8 0.0 copy-done
  32.8 3.4 %write_out.1 = (f32[32,4,128,128]{3,2,1,0:T(8,128)}, bf16[64,2048]{1,0:T(8,128)(2,1)}) custom-call(f32[32,4,128,128]{3,2,1,0:T(8,128)S(1)} %get-tuple-element.7.state, bf16[16,64,128]{2,1,0:T(8,128)(2,1)S(1)} %get-tuple-element.8.mixed_in, f32[16,2,128]{2,1,0:T(2,128)S(1)} %get-tuple-element.9.sums, f32[1,64]{1,0:T(1,128)S(1)} %bitcast.12), custom_call_target="tpu_custom_call" | custom-call | tf_op jit(solution)/shard_map/write_out/pallas_call | solution.py:463
Async XLA Ops:
  0.6 32.2 %copy-start = (f32[64]{0:T(128)S(1)}, f32[64]{0:T(128)}, u32[]{:S(2)}) copy-start(f32[64]{0:T(128)} %param.29) | copy-start | bytes 772

commit v6 on v5

--- a/solution.py
+++ b/solution.py
@@ -260,15 +260,16 @@
             proj[i] = out if g == 0 else proj[i] + out
 
     groups = n // 4
+    near = [g for g in (0, 1, 3, 2) if g < groups]
     for g in range(groups):
-        collect(g)
+        collect(near[g])
         if g == min(1, groups - 1):
             for c in load_w:
                 c.wait()
         if g > 1:
-            project(g - 2)
+            project(near[g - 2])
     for g in range(max(groups - 2, 0), groups):
-        project(g)
+        project(near[g])
     inverse = lax.rsqrt(jnp.sum(ssq[...], axis=1, keepdims=True) / width + 1e-06)
     beta_raw = scal[0] * inverse
     decay_raw = scal[1] * inverse
@@ -294,8 +295,8 @@
     lax.fori_loop(0, 8, recall_new, 0, unroll=2)
 
     def to_pair(h):
-        two = pl.ds(2 * h, 2)
-        return to_peer(att.at[0, two], att.at[1, two], asend, arecv, pair)
+        some = pl.ds(0, 3) if h == 2 else pl.ds(3, 1)
+        return to_peer(att.at[0, some], att.at[1, some], asend, arecv, pair)
 
     upper = core > 0
     for h in range(4):
@@ -314,8 +315,8 @@
         reads = grown * rq[h] + mm(seen.astype(BF16), rhs.astype(BF16))
         normed = reads * lax.rsqrt(jnp.mean(reads * reads, axis=-1, keepdims=True) + 1e-06)
         att[0, h] = (normed * gates[h]).astype(BF16)
-        if h % 2:
-            to_pair(h // 2).start()
+        if h > 1:
+            to_pair(h).start()
 
     def swap(slot, blocks):
         return pltpu.make_async_remote_copy(
@@ -325,22 +326,21 @@
 
     many = n // 4
 
-    def multiply(slot, side):
+    def multiply(slot, sides):
         attended = jnp.concatenate([att[slot, h] for h in range(4)], axis=1)
-        some = jnp.concatenate([wt[pl.ds(place(dz, side), 1)][0] for dz in [0] + far], axis=0)
-        out = mm_nt(some, attended).reshape(many, 128, 128)
-        blocks = pl.ds(side * many, many)
+        some = jnp.concatenate([wt[pl.ds(place(dz, side), 1)][0] for side in sides for dz in [0] + far], axis=0)
+        out = mm_nt(some, attended).reshape(many * len(sides), 128, 128)
+        blocks = pl.ds(sides[0] * many, many * len(sides))
         part[slot, blocks] = out
         psend[slot, blocks] = out.astype(BF16)
         swap(slot, blocks).start()
 
-    multiply(0, 0)
+    multiply(0, (0,))
     for dz in far:
         arrived(place(dz, 1))
-    multiply(0, 1)
+    multiply(0, (1,))
     to_peer(att.at[0], att.at[1], asend, arecv, pair).wait()
-    multiply(1, 0)
-    multiply(1, 1)
+    multiply(1, (0, 1))
 
     def send_sums(d):
         return to_peer(sums.at[me], sums.at[me], ssend, srecv, lax.rem(me + d, n))

time: 36.4 us -> 36.2 us (level)
  no operation moved by 1% of the time
where the time goes in v6:
time: 36.2 us; the launch traced here: 36.1 us
  Pallas kernels  35.4 us (98%)
  between operations  0.66 us (2%)
    pallas_call x1, Pallas kernels, local(): pl.pallas_call(functools.partial(main_kernel, n), out_shape=(VM(saved_sta...  32 us
    pallas_call x1, Pallas kernels, local(): pl.pallas_call(functools.partial(last_kernel, n), out_shape=(jax.ShapeDty...  3.43 us

profile of v6, /device:TPU:1, one launch (start us, length us, event | category | flops | bytes accessed | tf_op | source)
XLA Modules:
  0.0 36.1 jit_solution(3440337771355348614)
XLA Ops:
  0.6 0.0 copy-start
  0.6 32.0 %delta_step.1 = (f32[32,4,128,128]{3,2,1,0:T(8,128)S(1)}, bf16[16,64,128]{2,1,0:T(8,128)(2,1)S(1)}, f32[16,2,128]{2,1,0:T(2,128)S(1)}) custom-call(bf16[2048,128]{1,0:T(8,128)(2,1)} %tokens.1, bf16[512,128]{1,0:T(8,128)(2,1)} %out_w.1, f32[32,4,128,128]{3,2,1,0:T(8,128)} %saved.1, bf16[2048,512]{1,0:T(8,128)(2,1)} %wq.1, bf16[2048,512]{1,0:T(8,128)(2,1)} %wk.1, ...), custom_call_target="tpu_custom_call" | custom-call | tf_op jit(solution)/shard_map/delta_step/pallas_call | solution.py:411
  32.7 0.0 copy-done
  32.7 3.4 %write_out.1 = (f32[32,4,128,128]{3,2,1,0:T(8,128)}, bf16[64,2048]{1,0:T(8,128)(2,1)}) custom-call(f32[32,4,128,128]{3,2,1,0:T(8,128)S(1)} %get-tuple-element.7.state, bf16[16,64,128]{2,1,0:T(8,128)(2,1)S(1)} %get-tuple-element.8.mixed_in, f32[16,2,128]{2,1,0:T(2,128)S(1)} %get-tuple-element.9.sums, f32[1,64]{1,0:T(1,128)S(1)} %bitcast.12), custom_call_target="tpu_custom_call" | custom-call | tf_op jit(solution)/shard_map/write_out/pallas_call | solution.py:463
Async XLA Ops:
  0.6 32.0 %copy-start = (f32[64]{0:T(128)S(1)}, f32[64]{0:T(128)}, u32[]{:S(2)}) copy-start(f32[64]{0:T(128)} %param.29) | copy-start | bytes 772
